TPU v7x, 256 devices: a whole 4x4x8 slice. The times are simulated.
256 devices in a mesh: fs: 16 (over y, x), tp: 16 (over z, core).
Axes of the slice: x: 4, y: 4, z: 8, core: 2. Of those that a mesh axis runs over, the one named last changes fastest.
Arguments:
- tokens: bfloat16 [65536, 1024], P(('fs', 'tp')), may hold values from -6 to 6
- norm_in: float32 [1024], replicated, may hold values from 0.1 to 1.9
- value_weight: bfloat16 [1024, 2816], P('fs', 'tp'), may hold values from -0.1875 to 0.1875
- gate_weight: bfloat16 [1024, 2816], P('fs', 'tp'), may hold values from -0.1875 to 0.1875
- value_taps: float32 [3, 2816], P(None, 'tp'), may hold values from -3 to 3
- gate_taps: float32 [3, 2816], P(None, 'tp'), may hold values from -3 to 3
- down_weight: bfloat16 [2816, 1024], P('tp', 'fs'), may hold values from -0.109375 to 0.109375
- norm_out: float32 [1024], replicated, may hold values from 0.1 to 1.9
Outputs:
- mixed: bfloat16 [65536, 1024], P(('fs', 'tp'))
All inputs are finite; a program needn't handle non-finite values.
Results may differ from a plain program's by a relative error of at most 0.02.
Values may be sent and summed in bfloat16 or wider, within the bound.
A program may use at most 64 MiB of HBM per device.

v0:
```python
import jax
import jax.numpy as jnp
from jax import lax
from jax.sharding import Mesh
from jax.sharding import PartitionSpec as P

FS = ("fs_0", "fs_1")
FS_TP = ("fs_0", "fs_1", "tp")


norm_eps = 1e-06


def joined_along(blocks, dim):
    blocks = jnp.moveaxis(blocks, 0, dim)
    shape = blocks.shape
    return blocks.reshape(*shape[:dim], shape[dim] * shape[dim + 1], *shape[dim + 2 :])


def one_gather(arrays, axis, dims):
    line = jnp.concatenate([a.reshape(-1) for a in arrays])
    lines, at, done = lax.all_gather(line, axis), 0, []
    for a, dim in zip(arrays, dims):
        blocks = lines[:, at : at + a.size].reshape(-1, *a.shape)
        done.append(joined_along(blocks, dim))
        at += a.size
    return tuple(done)


def gathered_then(shard, axis, dim, work):
    return work(lax.all_gather(shard, axis, axis=dim, tiled=True), jnp.int32(0))


def shifted(value, axis, steps):
    count = lax.axis_size(axis)
    leading, last = max(0, -steps), min(count, count - steps)
    return lax.ppermute(value, axis, [(source, source + steps) for source in range(leading, last)])


def whole_of(array, axes, dim):
    if not axes:
        return array
    nearer = lax.all_gather(array, axes[-1], axis=dim, tiled=True)
    return whole_of(nearer, axes[:-1], dim)


def scattered(product, extent, axis):
    everything = product(jnp.int32(0), lax.axis_size(axis) * extent)
    own = lax.psum_scatter(everything.astype(jnp.bfloat16), axis, scatter_dimension=0, tiled=True)
    return own.astype(jnp.float32)


def normalize(values, scale):
    wide = values.astype(jnp.float32)
    power = jnp.mean(wide * wide, axis=-1, keepdims=True)
    return (wide * lax.rsqrt(power + norm_eps) * scale).astype(jnp.bfloat16)


def causal_conv(signal, earlier, taps):
    length = signal.shape[0]
    padded = jnp.concatenate([earlier, signal], axis=0).astype(jnp.float32)
    result = padded[0:length] * taps[0]
    result = result + padded[1 : length + 1] * taps[1]
    result = result + padded[2 : length + 2] * taps[2]
    return result


def shards(
    tokens, norm_in, value_weight, gate_weight, value_taps, gate_taps, down_weight, norm_out
):
    normed = normalize(tokens, norm_in)
    width = value_weight.shape[1]
    value_full, gate_full = one_gather((value_weight, gate_weight), FS, (0, 0))
    stacked = jnp.concatenate([value_full, gate_full], axis=1)

    def project(piece, start):
        return jnp.dot(piece, stacked, preferred_element_type=jnp.float32)

    joined = gathered_then(normed, "tp", 0, project)
    value_sum = joined[:, :width]
    gate_sum = joined[:, width:]
    value = value_sum.astype(jnp.bfloat16)
    gate = gate_sum.astype(jnp.bfloat16)
    edges = jnp.concatenate([value[-2:], gate[-2:]], axis=1)
    before = shifted(edges, FS, 1)
    conv_value = causal_conv(value, before[:, :width], value_taps)
    conv_gate = causal_conv(gate, before[:, width:], gate_taps)
    hidden = (jax.nn.gelu(conv_gate, approximate=True) * conv_value).astype(jnp.bfloat16)
    down_full = whole_of(down_weight, FS, 1)

    def partial_value(start, count):
        picked = lax.dynamic_slice_in_dim(hidden, start, count, 0)
        return jnp.dot(picked, down_full, preferred_element_type=jnp.float32)

    projected = scattered(partial_value, tokens.shape[0], "tp")
    return normalize(projected, norm_out)


def solution(mesh):
    split = Mesh(mesh.devices.reshape(4, 4, mesh.shape["tp"]), ("fs_0", "fs_1", "tp"))
    return jax.shard_map(
        shards,
        mesh=split,
        in_specs=(
            P(FS_TP, None),
            P(),
            P(FS, "tp"),
            P(FS, "tp"),
            P(None, "tp"),
            P(None, "tp"),
            P("tp", FS),
            P(),
        ),
        out_specs=P(FS_TP, None),
        check_vma=False,
    )
```

profile of v0, /device:TPU:1, one launch (start us, length us, event | category | flops | bytes accessed | tf_op | source)
XLA Modules:
  0.0 170.5 jit_solution(15165111547059668911)
XLA Ops:
  6.5 0.0 all-gather.3.cloned.1.call-start
  6.5 1.2 fusion.24
  7.8 2.0 %fusion.26 = bf16[256,1024]{1,0:T(8,128)(2,1)} fusion(bf16[256,1024]{1,0:T(8,128)(2,1)} %param.8, f32[1024]{0:T(1024)} %param.9, f32[256]{0:T(256)S(1)} %add_rsqrt_fusion.1), kind=kLoop, calls=%fused_computation.40 | loop fusion | flops 1048576 | bytes 1053696 | tf_op jit(solution)/shard_map/convert_element_type | solution.py:56
  9.8 0.0 all-gather.3.cloned.1.call-update
  9.8 0.0 copy-start
  9.8 0.0 reduce-scatter.2.cloned.1.call-start
  9.9 0.9 reshape.24
  10.8 0.9 reshape.25
  11.6 21.1 %all-gather = bf16[360448]{0:T(1024)(128)(2,1)S(1)} all-gather(bf16[22528]{0:T(1024)(128)(2,1)S(1)} %pad_maximum_fusion), channel_id=2, replica_groups=mesh['fs_0'=4,'fs_1'=4,'tp'=16] {'fs_0','fs_1'}, dimensions={0}, use_global_device_ids=true | all-gather | bytes 765952 | tf_op jit(solution)/shard_map/all_gather | solution.py:22
  32.7 0.0 copy-start.2
  32.7 0.0 copy-start.3
  32.7 0.3 reshape.26
  33.1 1.0 reshape_reshape.6
  34.1 1.0 reshape_reshape.7
  35.1 0.0 copy-done
  35.1 10.4 %all_gather.18 = bf16[176,256]{0,1:T(8,128)(2,1)S(1)} all-gather(bf16[176,64]{0,1:T(8,128)(2,1)S(1)} %copy-done), channel_id=1, replica_groups=mesh['fs_0'=4,'fs_1'=4,'tp'=16] {'fs_1'}, dimensions={1}, use_global_device_ids=true | all-gather | bytes 112640 | tf_op jit(solution)/shard_map/all_gather | solution.py:43
  45.5 11.1 %all_gather.19 = bf16[176,1024]{0,1:T(8,128)(2,1)S(1)} all-gather(bf16[176,256]{0,1:T(8,128)(2,1)S(1)} %all_gather.18), channel_id=1, replica_groups=mesh['fs_0'=4,'fs_1'=4,'tp'=16] {'fs_0'}, dimensions={1}, use_global_device_ids=true | all-gather | bytes 450560 | tf_op jit(solution)/shard_map/all_gather | solution.py:43
  56.6 0.0 copy-done.2
  56.6 0.0 copy-done.3
  56.6 13.3 %all-gather.3.cloned.1.call-done = bf16[4096,1024]{1,0:T(8,128)(2,1)} async-done(((bf16[256,1024]{1,0:T(8,128)(2,1)}), bf16[4096,1024]{1,0:T(8,128)(2,1)}) %all-gather.3.cloned.1.call-update) | async-done | bytes 8388624 | tf_op jit(solution)/shard_map/all_gather | solution.py:31
  69.9 6.7 %convolution_convert_fusion.1 = bf16[4096,352]{0,1:T(8,128)(2,1)S(1)} fusion(bf16[4096,1024]{1,0:T(8,128)(2,1)} %all-gather.3.cloned.1.call-done, bf16[1024,176]{1,0:T(8,128)(2,1)S(1)} %reshape_reshape.7, bf16[1024,176]{1,0:T(8,128)(2,1)S(1)} %reshape_reshape.6), kind=kOutput, calls=%fused_computation.1 | convolution fusion | flops 2955673600 | bytes 11993088 | tf_op jit(solution)/shard_map/dot_general | solution.py:77
  76.6 0.1 slice.87
  76.7 3.3 %collective-permute-start = (bf16[2,352]{0,1:T(8,128)(2,1)S(1)}, bf16[2,352]{0,1:T(8,128)(2,1)S(1)}, u32[]{:S(2)}, u32[]{:S(2)}) collective-permute-start(bf16[2,352]{0,1:T(8,128)(2,1)S(1)} %slice.87), channel_id=1, source_target_pairs={{0,16},{16,32},{32,48},{48,64},{64,80},{80,96},{96,112},{112,128},... | collective-permute-start | bytes 4232 | tf_op jit(solution)/shard_map/ppermute | solution.py:37
  80.0 0.2 fusion.38
  80.2 1.2 collective-permute-done
  81.3 1.6 maximum_convert_fusion
  82.9 9.3 %convolution_convert_fusion = bf16[4096,1024]{1,0:T(8,128)(2,1)} fusion(bf16[176,1024]{0,1:T(8,128)(2,1)S(1)} %all_gather.19, f32[4098,176]{0,1:T(8,128)S(1)} %get-tuple-element.18, f32[4098,176]{0,1:T(8,128)S(1)} %get-tuple-element.17, f32[176]{0:T(256)S(1)} %bitcast.9, f32[176]{0:T(256)S(1)} %bitcast.10, f32[176]{0:T(256)S(1)} %bitcast.8, ...), kind=kOutput, calls=%fused_computation | convolution fusion | flops 1495007232 | bytes 26220544 | tf_op jit(solution)/shard_map/dot_general | solution.py:93
  92.2 0.0 copy-start.1
  92.2 0.0 reduce-scatter.2.cloned.1.call-update
  92.2 68.1 %reduce-scatter.2.cloned.1.call-done = bf16[256,1024]{1,0:T(8,128)(2,1)} async-done(((bf16[4096,1024]{1,0:T(8,128)(2,1)}), bf16[256,1024]{1,0:T(8,128)(2,1)}) %reduce-scatter.2.cloned.1.call-update) | async-done | bytes 524304 | tf_op jit(solution)/shard_map/reduce_scatter | solution.py:49
  160.4 1.2 fusion.27
  161.6 0.0 copy-done.1
  161.6 2.0 %fusion.29 = bf16[256,1024]{1,0:T(8,128)(2,1)} fusion(bf16[256,1024]{1,0:T(8,128)(2,1)} %reduce-scatter.2.cloned.1.call-done, f32[1024]{0:T(1024)S(1)} %copy-done.1, f32[256]{0:T(256)S(1)} %add_rsqrt_fusion), kind=kLoop, calls=%fused_computation.43 | loop fusion | flops 1048576 | bytes 1053696 | tf_op jit(solution)/shard_map/convert_element_type | solution.py:56
  (7 shorter events, 0.1 us)
Async XLA Ops:
  6.5 63.4 %all-gather.3.cloned.1.call-start = ((), (), s32[]{:S(2)}) async-start(), calls=%async_computation.1 | async-start | bytes 8912896 | tf_op jit(solution)/shard_map/all_gather | solution.py:31
  9.8 25.3 %copy-start = (bf16[176,64]{0,1:T(8,128)(2,1)S(1)}, bf16[176,64]{0,1:T(8,128)(2,1)}, u32[]{:S(2)}) copy-start(bf16[176,64]{0,1:T(8,128)(2,1)} %param.14) | copy-start | bytes 67588
  9.8 150.5 %reduce-scatter.2.cloned.1.call-start = ((), (), s32[]{:S(2)}) async-start(), calls=%async_computation.2 | async-start | bytes 8912896 | tf_op jit(solution)/shard_map/reduce_scatter | solution.py:49
  32.7 23.9 %copy-start.2 = (f32[3,176]{1,0:T(4,128)S(1)}, f32[3,176]{1,0:T(4,128)}, u32[]{:S(2)}) copy-start(f32[3,176]{1,0:T(4,128)} %param.12) | copy-start | bytes 6340
  32.7 23.9 %copy-start.3 = (f32[3,176]{1,0:T(4,128)S(1)}, f32[3,176]{1,0:T(4,128)}, u32[]{:S(2)}) copy-start(f32[3,176]{1,0:T(4,128)} %param.13) | copy-start | bytes 6340
  76.7 4.6 %collective-permute-start = (bf16[2,352]{0,1:T(8,128)(2,1)S(1)}, bf16[2,352]{0,1:T(8,128)(2,1)S(1)}, u32[]{:S(2)}, u32[]{:S(2)}) collective-permute-start(bf16[2,352]{0,1:T(8,128)(2,1)S(1)} %slice.87), channel_id=1, source_target_pairs={{0,16},{16,32},{32,48},{48,64},{64,80},{80,96},{96,112},{112,128},... | collective-permute-start | bytes 4232 | tf_op jit(solution)/shard_map/ppermute | solution.py:37
  92.2 69.4 %copy-start.1 = (f32[1024]{0:T(1024)S(1)}, f32[1024]{0:T(1024)}, u32[]{:S(2)}) copy-start(f32[1024]{0:T(1024)} %param.15) | copy-start | bytes 12292
Sparse Core Ops, SparseCore 0:
  9.9 59.9 all-gather.2
  92.3 67.9 reduce-scatter.1
where the time goes:
time: 173 us; the launch traced here: 170 us
  waiting for transfers between devices  82.6 us (48%)
  blocking collectives  42.6 us (25%)
  matrix products  15.9 us (9%)
  between operations  13.5 us (8%)
  other arithmetic  8.1 us (5%)
  local copies, waits for them, and re-layouts  4.42 us (3%)
  starting transfers between devices  3.32 us (2%)
    reduce_scatter x1, waiting for transfers between devices, scattered(): lax.psum_scatter(everything.astype(jnp.bfloat16), axis, scatter_dimension...  68.1 us
    all_gather x2, blocking collectives, whole_of(): nearer = lax.all_gather(array, axes[-1], axis=dim, tiled=True)  21.5 us
    all_gather x1, blocking collectives, one_gather(): lines, at, done = (lax.all_gather(line, axis), 0, [])  21.1 us
    all_gather x1, waiting for transfers between devices, gathered_then(): return work(lax.all_gather(shard, axis, axis=dim, tiled=True), jnp.int32(0))  13.3 us
    dot_general x1, matrix products, partial_value(): return jnp.dot(picked, down_full, preferred_element_type=jnp.float32)  9.25 us
    dot_general x1, matrix products, project(): return jnp.dot(piece, stacked, preferred_element_type=jnp.float32)  6.67 us
    convert_element_type x2, other arithmetic, normalize(): return (wide * lax.rsqrt(power + norm_eps) * scale).astype(jnp.bfloat16)  4.06 us
  transfers between devices with their start and end apart: 3, of which 3 were waited for; matrix products, arithmetic and copies ran while one was open for 3% of the time, Pallas kernels for 0%

commit v1 on v0

v1 whole, which is shorter than its diff:
```python
import functools

import jax
import jax.numpy as jnp
from jax import lax
from jax.experimental import pallas as pl
from jax.experimental.pallas import tpu as pltpu
from jax.sharding import Mesh
from jax.sharding import PartitionSpec as P

FS = ("y", "x")
ALL = ("y", "x", "z", "core")
GATHER = ("y", "x", "z")

norm_eps = 1e-06
HALO = 16
LANES = 128


def packed_up(value, gate):
    tail = value.shape[1] - LANES
    pad = jnp.zeros((value.shape[0], LANES // 2 - tail), value.dtype)
    return jnp.concatenate(
        [value[:, :LANES], gate[:, :LANES], value[:, LANES:], pad, gate[:, LANES:], pad],
        axis=1,
    )


def normalized(wide, scale):
    power = jnp.mean(wide * wide, axis=-1, keepdims=True)
    return wide * lax.rsqrt(power + norm_eps) * scale


def ffn_kernel(tokens_ref, scale_ref, up_ref, down_ref, taps_ref, out_ref, normed, upped):
    step = pl.program_id(0)
    rows = out_ref.shape[0]

    @pl.when(step == 0)
    def _():
        wide = tokens_ref[...].astype(jnp.float32)
        normed[...] = normalized(wide, scale_ref[...]).astype(jnp.bfloat16)
        out_ref[...] = jnp.zeros_like(out_ref)

    weights = up_ref[...].reshape(-1, 3 * LANES)
    upped[...] = jnp.dot(normed[...], weights, preferred_element_type=jnp.float32)
    taps = taps_ref[0]
    conv = upped[pl.ds(HALO - 2, rows), :] * taps[0:1]
    conv = conv + upped[pl.ds(HALO - 1, rows), :] * taps[1:2]
    conv = conv + upped[pl.ds(HALO, rows), :] * taps[2:3]
    last = conv[:, 2 * LANES :]
    main = jax.nn.gelu(conv[:, LANES : 2 * LANES], approximate=True) * conv[:, :LANES]
    rest = jax.nn.gelu(pltpu.roll(last, LANES // 2, 1), approximate=True) * last
    hidden = jnp.concatenate([main, rest], axis=1).astype(jnp.bfloat16)
    half = down_ref.shape[2]
    blocks = down_ref[...].reshape(-1, 2 * half, LANES)
    down = jnp.concatenate([blocks[i] for i in range(blocks.shape[0])], axis=1)
    out_ref[...] += jnp.dot(
        hidden[:, : 2 * half], down, preferred_element_type=jnp.float32
    )


def swapped(value, axis):
    return lax.ppermute(value, axis, [(i, i ^ 1) for i in range(lax.axis_size(axis))])


def shards(
    tokens, norm_in, value_weight, gate_weight, value_taps, gate_taps, down_weight, norm_out
):
    count = lax.axis_size(ALL)
    core = lax.axis_index("core")
    rows = tokens.shape[0]
    halo = lax.ppermute(tokens[-HALO:], ALL, [(i, i + 1) for i in range(count - 1)])
    other = swapped(tokens, "core")
    before = jnp.where(core == 0, halo, swapped(halo, "core"))
    first = jnp.where(core == 0, tokens, other)
    second = jnp.where(core == 0, other, tokens)
    block = jnp.concatenate([before, first, second], axis=0)

    up = packed_up(value_weight, gate_weight)
    up_all = lax.all_gather(up, GATHER)
    groups = count // 2
    depth = lax.axis_size("z")
    up_all = up_all.reshape(groups // depth, depth, *up.shape)

    even = lax.rem(lax.axis_index("x"), 2) == 0
    partner = swapped(down_weight, "x")
    left = jnp.where(even, down_weight, partner)
    right = jnp.where(even, partner, down_weight)
    pair = jnp.concatenate([left, right], axis=1)
    pair = jnp.pad(pair, ((0, 192 - pair.shape[0]), (0, 0)))
    own = jnp.where(even, pair[:96], pair[96:])
    down_all = lax.all_gather(own, GATHER).reshape(groups // depth, depth, *own.shape)

    taps = packed_up(value_taps, gate_taps)
    taps_all = lax.all_gather(taps, "z")

    wide = rows * 2
    spec = pl.BlockSpec
    partial = pl.pallas_call(
        ffn_kernel,
        grid=(depth,),
        in_specs=[
            spec((wide + HALO, tokens.shape[1]), lambda i: (0, 0)),
            spec((1, tokens.shape[1]), lambda i: (0, 0)),
            spec((groups // depth, 1, *up.shape), lambda i: (0, i, 0, 0)),
            spec((groups // depth, 1, *own.shape), lambda i: (0, i, 0, 0)),
            spec((1, *taps.shape), lambda i: (i, 0, 0)),
        ],
        out_specs=spec((wide, tokens.shape[1]), lambda i: (0, 0)),
        out_shape=jax.ShapeDtypeStruct((wide, tokens.shape[1]), jnp.float32),
        scratch_shapes=[
            pltpu.VMEM((wide + HALO, tokens.shape[1]), jnp.bfloat16),
            pltpu.VMEM((wide + HALO, 3 * LANES), jnp.float32),
        ],
        compiler_params=pltpu.CompilerParams(vmem_limit_bytes=48 * 2**20),
        cost_estimate=pl.CostEstimate(
            flops=5 * 10**9, bytes_accessed=12 * 10**6, transcendentals=10**6
        ),
    )(block, norm_in[None], up_all, down_all, taps_all)

    mine = jnp.where(core == 0, partial[:rows], partial[rows:])
    theirs = jnp.where(core == 0, partial[rows:], partial[:rows]).astype(jnp.bfloat16)
    total = mine + swapped(theirs, "core").astype(jnp.float32)
    return normalized(total, norm_out).astype(jnp.bfloat16)


def solution(mesh):
    split = Mesh(mesh.devices.reshape(4, 4, 8, 2), ALL)
    return jax.shard_map(
        shards,
        mesh=split,
        in_specs=(
            P(ALL, None),
            P(),
            P(FS, ("z", "core")),
            P(FS, ("z", "core")),
            P(None, ("z", "core")),
            P(None, ("z", "core")),
            P(("z", "core"), FS),
            P(),
        ),
        out_specs=P(ALL, None),
        check_vma=False,
    )
```

time: 173 us -> 277 us (1.60)
  waiting for transfers between devices: 82.6 us -> 202 us
  blocking collectives: 42.6 us -> 23.4 us
  matrix products: 15.9 us -> 0 us
  Pallas kernels: 0 us -> 13.4 us
  starting transfers between devices: 3.32 us -> 12.6 us
  other arithmetic: 8.1 us -> 3.41 us
  local copies, waits for them, and re-layouts: 4.42 us -> 8.07 us
    all_gather x1 -> x2, waiting for transfers between devices: 13.3 us -> 198 us  [the longest x1 121 us: shards(): up_all = lax.all_gather(up, GATHER)]
    reduce_scatter x1 -> x0, waiting for transfers between devices: 68.1 us -> none  [scattered(): lax.psum_scatter(everything.astype(jnp.bfloat16), axis, scatter_dimension...]
    all_gather x3 -> x1, blocking collectives: 42.6 us -> 23.4 us  [shards(): taps_all = lax.all_gather(taps, 'z')]
    dot_general x2 -> x0, matrix products: 15.9 us -> none  [the longest x1 9.25 us: partial_value(): return jnp.dot(picked, down_full, preferred_element_type=jnp.float32)]
    pallas_call x0 -> x1, Pallas kernels: none -> 13.4 us  [shards(): pl.pallas_call(ffn_kernel, grid=(depth,), in_specs=[spec((wide + HALO, to...]
    ppermute x1 -> x5, starting transfers between devices: 3.28 us -> 12.6 us  [the longest x4 10.7 us: swapped(): lax.ppermute(value, axis, [(i, i ^ 1) for i in range(lax.axis_size(axis))])]
    slice x5 -> x9, local copies, waits for them, and re-layouts: 0.25 us -> 6.37 us  [the longest x2 1.4 us: packed_up(): value[:, LANES:]]
    convert_element_type x3 -> x2, other arithmetic: 5.63 us -> 1.13 us  [the longest x1 1.04 us: shards(): return normalized(total, norm_out).astype(jnp.bfloat16)]
  transfers between devices with their start and end apart: 3 -> 7, of which waited for: 3 -> 5; matrix products, arithmetic and copies ran while one was open for 3% -> 3% of each run, Pallas kernels for 0% -> 0%
where the time goes in v1:
time: 277 us; the launch traced here: 276 us
  waiting for transfers between devices  202 us (73%)
  blocking collectives  23.4 us (8%)
  between operations  13.5 us (5%)
  Pallas kernels  13.4 us (5%)
  starting transfers between devices  12.6 us (5%)
  local copies, waits for them, and re-layouts  8.07 us (3%)
  other arithmetic  3.41 us (1%)
    all_gather x1, waiting for transfers between devices, shards(): up_all = lax.all_gather(up, GATHER)  121 us
    all_gather x1, waiting for transfers between devices, shards(): lax.all_gather(own, GATHER).reshape(groups // depth, depth, *own.shape)  76.3 us
    all_gather x1, blocking collectives, shards(): taps_all = lax.all_gather(taps, 'z')  23.4 us
    pallas_call x1, Pallas kernels, shards(): pl.pallas_call(ffn_kernel, grid=(depth,), in_specs=[spec((wide + HALO, to...  13.4 us
    ppermute x4, starting transfers between devices, swapped(): lax.ppermute(value, axis, [(i, i ^ 1) for i in range(lax.axis_size(axis))])  10.7 us
  transfers between devices with their start and end apart: 7, of which 5 were waited for; matrix products, arithmetic and copies ran while one was open for 3% of the time, Pallas kernels for 0%

profile of v1, /device:TPU:1, one launch (start us, length us, event | category | flops | bytes accessed | tf_op | source)
XLA Modules:
  0.0 276.4 jit_solution(3531159418216786259)
XLA Ops:
  6.5 0.0 all-gather.9.cloned.1.call-start
  6.5 0.9 copy.11
  7.4 2.1 collective-permute-start.3
  9.5 1.4 collective-permute-done.3
  11.0 0.1 pad_maximum_fusion.1
  11.1 0.7 fusion.1
  11.8 0.0 all-gather.9.cloned.1.call-update
  11.8 0.0 all-gather.7.cloned.1.call-start
  11.8 0.7 slice.45
  12.6 0.7 slice.43
  13.3 0.7 slice.46
  14.0 0.7 slice.44
  14.7 0.7 concatenate.13
  15.5 0.0 all-gather.7.cloned.1.call-update
  15.5 3.8 %collective-permute-start.2 = (bf16[256,1024]{1,0:T(8,128)(2,1)}, bf16[256,1024]{1,0:T(8,128)(2,1)S(1)}, u32[]{:S(2)}, u32[]{:S(2)}) collective-permute-start(bf16[256,1024]{1,0:T(8,128)(2,1)} %param.8), channel_id=1, source_target_pairs={{0,1},{1,0},{2,3},{3,2},{4,5},{5,4},{6,7},{7,6},{8,9},{9,8},{10,11... | collective-permute-start | bytes 1572872 | tf_op jit(solution)/shard_map/ppermute | solution.py:63
  19.3 0.8 slice.42
  20.1 1.9 collective-permute-start
  22.0 1.2 collective-permute-done
  23.2 0.2 collective-permute-start.1
  23.3 0.7 slice.51
  24.0 0.7 slice.49
  24.7 0.7 slice.52
  25.4 0.7 slice.50
  26.1 0.1 concatenate.15
  26.2 23.4 %all-gather.3.taps_ref = f32[8,3,384]{2,1,0:T(4,128)S(1)} all-gather(f32[1,3,384]{2,1,0:T(4,128)S(1)} %bitcast.5), channel_id=4, replica_groups=mesh['y'=4,'x'=4,'z'=8,'core'=2] {'z'}, dimensions={0}, use_global_device_ids=true | all-gather | bytes 41472 | tf_op jit(solution)/shard_map/all_gather | solution.py:95
  49.6 0.0 collective-permute-done.1
  49.6 0.0 copy-start
  49.6 0.0 collective-permute-done.2
  49.6 1.1 broadcast_select_fusion.1
  50.8 0.1 pad_maximum_fusion.tokens_ref
  50.8 76.3 %all-gather.9.cloned.1.call-done = bf16[12288,128]{1,0:T(8,128)(2,1)} async-done(((bf16[96,128]{1,0:T(8,128)(2,1)}), bf16[12288,128]{1,0:T(8,128)(2,1)}) %all-gather.9.cloned.1.call-update) | async-done | bytes 3145744 | tf_op jit(solution)/shard_map/all_gather | solution.py:92
  127.1 121.5 %all-gather.7.cloned.1.call-done = bf16[8192,384]{1,0:T(8,128)(2,1)} async-done(((bf16[64,384]{1,0:T(8,128)(2,1)}), bf16[8192,384]{1,0:T(8,128)(2,1)}) %all-gather.7.cloned.1.call-update) | async-done | bytes 6291472 | tf_op jit(solution)/shard_map/all_gather | solution.py:80
  248.6 0.0 copy-done
  248.6 13.4 %shard_map.82 = f32[512,1024]{1,0:T(8,128)S(1)} custom-call(bf16[528,1024]{1,0:T(8,128)(2,1)S(1)} %pad_maximum_fusion.tokens_ref, f32[1,1024]{1,0:T(1,128)S(1)} %bitcast.4, bf16[16,8,64,384]{3,2,1,0:T(8,128)(2,1)} %bitcast.6, bf16[16,8,96,128]{3,2,1,0:T(8,128)(2,1)} %bitcast.7, f32[8,3,384]{2,1,0:T(4,128)S(1)} %all-gather.3.taps_ref), custom_call_target="tpu_custom_call" | custom-call | flops 5000000000 | bytes 12000000 | tf_op jit(solution)/shard_map/pallas_call | solution.py:99
  262.0 0.0 copy-start.1
  262.0 0.1 select_convert_fusion
  262.1 4.6 %collective-permute-start.4 = (bf16[256,1024]{1,0:T(8,128)(2,1)S(1)}, bf16[256,1024]{1,0:T(8,128)(2,1)S(1)}, u32[]{:S(2)}, u32[]{:S(2)}) collective-permute-start(bf16[256,1024]{1,0:T(8,128)(2,1)S(1)} %select_convert_fusion), channel_id=1, source_target_pairs={{0,1},{1,0},{2,3},{3,2},{4,5},{5,4},{6,7},{7,6},{8,9},{9,8},{10,11... | collective-permute-start | bytes 1572872 | tf_op jit(solution)/shard_map/ppermute | solution.py:63
  266.7 1.5 collective-permute-done.4
  268.2 0.3 multiply_reduce_fusion
  268.5 0.0 copy-done.1
  268.5 1.0 multiply_convert_fusion
  (5 shorter events, 0.0 us)
Async XLA Ops:
  6.5 120.6 %all-gather.9.cloned.1.call-start = ((), (), s32[]{:S(2)}) async-start(), calls=%async_computation.1 | async-start | bytes 3170304 | tf_op jit(solution)/shard_map/all_gather | solution.py:92
  7.4 3.6 %collective-permute-start.3 = (bf16[176,64]{1,0:T(8,128)(2,1)S(1)}, bf16[176,64]{1,0:T(8,128)(2,1)S(1)}, u32[]{:S(2)}, u32[]{:S(2)}) collective-permute-start(bf16[176,64]{1,0:T(8,128)(2,1)S(1)} %copy.11), channel_id=1, source_target_pairs={{0,16},{16,0},{32,48},{48,32},{1,17},{17,1},{33,49},{49,33},{2,18}... | collective-permute-start | bytes 67592 | tf_op jit(solution)/shard_map/ppermute | solution.py:63
  11.8 236.8 %all-gather.7.cloned.1.call-start = ((), (), s32[]{:S(2)}) async-start(), calls=%async_computation | async-start | bytes 6340608 | tf_op jit(solution)/shard_map/all_gather | solution.py:80
  15.5 34.2 %collective-permute-start.2 = (bf16[256,1024]{1,0:T(8,128)(2,1)}, bf16[256,1024]{1,0:T(8,128)(2,1)S(1)}, u32[]{:S(2)}, u32[]{:S(2)}) collective-permute-start(bf16[256,1024]{1,0:T(8,128)(2,1)} %param.8), channel_id=1, source_target_pairs={{0,1},{1,0},{2,3},{3,2},{4,5},{5,4},{6,7},{7,6},{8,9},{9,8},{10,11... | collective-permute-start | bytes 1572872 | tf_op jit(solution)/shard_map/ppermute | solution.py:63
  20.1 3.1 %collective-permute-start = (bf16[16,1024]{1,0:T(8,128)(2,1)S(1)}, bf16[16,1024]{1,0:T(8,128)(2,1)S(1)}, u32[]{:S(2)}, u32[]{:S(2)}) collective-permute-start(bf16[16,1024]{1,0:T(8,128)(2,1)S(1)} %slice.42), channel_id=1, source_target_pairs={{0,1},{1,2},{2,3},{3,4},{4,5},{5,6},{6,7},{7,8},{8,9},{9,10},{10,1... | collective-permute-start | bytes 98312 | tf_op jit(solution)/shard_map/ppermute | solution.py:72
  23.2 26.4 %collective-permute-start.1 = (bf16[16,1024]{1,0:T(8,128)(2,1)S(1)}, bf16[16,1024]{1,0:T(8,128)(2,1)S(1)}, u32[]{:S(2)}, u32[]{:S(2)}) collective-permute-start(bf16[16,1024]{1,0:T(8,128)(2,1)S(1)} %collective-permute-done), channel_id=1, source_target_pairs={{0,1},{1,0},{2,3},{3,2},{4,5},{5,4},{6,7},{7,6},{8,9},{9,8},{10,11... | collective-permute-start | bytes 98312 | tf_op jit(solution)/shard_map/ppermute | solution.py:63
  49.6 199.0 %copy-start = (f32[1024]{0:T(1024)S(1)}, f32[1024]{0:T(1024)}, u32[]{:S(2)}) copy-start(f32[1024]{0:T(1024)} %param.9) | copy-start | bytes 12292
  262.0 6.5 %copy-start.1 = (f32[1024]{0:T(1024)S(1)}, f32[1024]{0:T(1024)}, u32[]{:S(2)}) copy-start(f32[1024]{0:T(1024)} %param.15) | copy-start | bytes 12292
  262.1 6.1 %collective-permute-start.4 = (bf16[256,1024]{1,0:T(8,128)(2,1)S(1)}, bf16[256,1024]{1,0:T(8,128)(2,1)S(1)}, u32[]{:S(2)}, u32[]{:S(2)}) collective-permute-start(bf16[256,1024]{1,0:T(8,128)(2,1)S(1)} %select_convert_fusion), channel_id=1, source_target_pairs={{0,1},{1,0},{2,3},{3,2},{4,5},{5,4},{6,7},{7,6},{8,9},{9,8},{10,11... | collective-permute-start | bytes 1572872 | tf_op jit(solution)/shard_map/ppermute | solution.py:63
Sparse Core Ops, SparseCore 0:
  11.9 115.1 all-gather.8
  130.8 117.7 all-gather.6

commit v2 on v1

v2 whole, which is shorter than its diff:
```python
import jax
import jax.numpy as jnp
from jax import lax
from jax.experimental import pallas as pl
from jax.experimental.pallas import tpu as pltpu
from jax.sharding import Mesh
from jax.sharding import PartitionSpec as P

FS = ("y", "x")
ALL = ("y", "x", "z", "core")
MESH = pl.DeviceIdType.MESH
DMA = pltpu.SemaphoreType.DMA

norm_eps = 1e-06
HALO = 16
LANES = 128
NX = NY = 4
NZ = 8
PART = 32


def packed_up(value, gate):
    tail = value.shape[1] - LANES
    pad = jnp.zeros((value.shape[0], LANES // 2 - tail), value.dtype)
    return jnp.concatenate(
        [value[:, :LANES], gate[:, :LANES], value[:, LANES:], pad, gate[:, LANES:], pad],
        axis=1,
    )


def packed_down(down):
    half = 96
    pad = jnp.zeros((2 * half - down.shape[0], down.shape[1]), down.dtype)
    low = jnp.concatenate([down[half:], pad], axis=0)
    return jnp.concatenate([down[:half], low], axis=1)


def normalized(wide, scale):
    power = jnp.mean(wide * wide, axis=-1, keepdims=True)
    return wide * lax.rsqrt(power + norm_eps) * scale


def moved(ref, send, recv, to):
    return pltpu.make_async_remote_copy(
        src_ref=ref, dst_ref=ref, send_sem=send, recv_sem=recv, device_id=to, device_id_type=MESH
    )


def kernel(
    tokens_ref,
    norm_in_ref,
    value_ref,
    gate_ref,
    value_taps_ref,
    gate_taps_ref,
    down_ref,
    norm_out_ref,
    out_ref,
    up_all,
    down_all,
    taps_all,
    rows_all,
    halo,
    normed,
    upped,
    total,
    leaving,
    arriving,
    uz_s, uz_r, tz_s, tz_r,
    ay_s, ay_r, bx_s, bx_r,
    ax_s, ax_r, by_s, by_r,
    dx_s, dx_r, dy_s, dy_r,
    dz_s, dz_r,
    pair_s, pair_r, halo_s, halo_r, sum_s, sum_r,
):
    y, x, z, core = (lax.axis_index(name) for name in ALL)
    rows = out_ref.shape[0]
    x_up, x_down, x_far = (lax.rem(x + k, NX) for k in (1, 3, 2))
    y_up, y_down, y_far = (lax.rem(y + k, NY) for k in (1, 3, 2))
    z_up, z_down = lax.rem(z + 1, NZ), lax.rem(z + NZ - 1, NZ)
    to_xu, to_xd = {"x": x_up}, {"x": x_down}
    to_yu, to_yd = {"y": y_up}, {"y": y_down}
    to_zu, to_zd = {"z": z_up}, {"z": z_down}
    to_pair = {"core": 1 - core}
    z_wrap = (z + 1) // NZ
    x_wrap = (x + z_wrap) // NX
    to_next = {"z": z_up, "x": lax.rem(x + z_wrap, NX), "y": lax.rem(y + x_wrap, NY)}
    z_back = 1 - (z + NZ - 1) // NZ
    x_back = 1 - (x + NX - z_back) // NX
    to_prev = {"z": z_down, "x": lax.rem(x + NX - z_back, NX), "y": lax.rem(y + NY - x_back, NY)}

    up_all[z, y, x] = packed_up(value_ref[...], gate_ref[...])
    down_all[z, y, x] = packed_down(down_ref[...])
    taps_all[z, 0:3] = packed_up(value_taps_ref[...], gate_taps_ref[...])
    rows_all[core] = tokens_ref[...]

    barrier = pltpu.get_barrier_semaphore()
    for device in (to_xu, to_xd, to_yu, to_yd, to_zu, to_zd, to_pair, to_prev):
        pl.semaphore_signal(barrier, inc=1, device_id=device, device_id_type=MESH)
    pl.semaphore_wait(barrier, 8)

    def block(i):
        step = (i + 1) // 2
        return lax.rem(z + NZ + step - 2 * step * lax.rem(i, 2), NZ)

    def uz(i, b, to):
        return [moved(up_all.at[b, y, x], uz_s.at[i], uz_r.at[i], to),
                moved(taps_all.at[b], tz_s.at[i], tz_r.at[i], to)]

    def uz_half(i, b, lo, to):
        half = [moved(up_all.at[b, y, x, pl.ds(lo, PART)], uz_s.at[i], uz_r.at[i], to)]
        return half + ([moved(taps_all.at[b], tz_s.at[i], tz_r.at[i], to)] if lo == 0 else [])

    def first(i, b, yu, yd, xu, xd):
        return [
            moved(up_all.at[b, yu, x, pl.ds(0, PART)], ay_s.at[i, 0], ay_r.at[i, 0], to_yu),
            moved(up_all.at[b, yd, x, pl.ds(0, PART)], ay_s.at[i, 1], ay_r.at[i, 1], to_yd),
            moved(up_all.at[b, y, xu, pl.ds(PART, PART)], bx_s.at[i, 0], bx_r.at[i, 0], to_xu),
            moved(up_all.at[b, y, xd, pl.ds(PART, PART)], bx_s.at[i, 1], bx_r.at[i, 1], to_xd),
        ]

    def first_far(i, b, yu, yd, xu, xd):
        h = PART // 2
        return [
            moved(up_all.at[b, yu, x, pl.ds(0, h)], ay_s.at[i, 2], ay_r.at[i, 2], to_yu),
            moved(up_all.at[b, yd, x, pl.ds(h, h)], ay_s.at[i, 3], ay_r.at[i, 3], to_yd),
            moved(up_all.at[b, y, xu, pl.ds(PART, h)], bx_s.at[i, 2], bx_r.at[i, 2], to_xu),
            moved(up_all.at[b, y, xd, pl.ds(PART + h, h)], bx_s.at[i, 3], bx_r.at[i, 3], to_xd),
        ]

    def last(i, b, yu, yd, xu, xd):
        return [
            moved(up_all.at[b, :, xu, pl.ds(0, PART)], ax_s.at[i, 0], ax_r.at[i, 0], to_xu),
            moved(up_all.at[b, :, xd, pl.ds(0, PART)], ax_s.at[i, 1], ax_r.at[i, 1], to_xd),
            moved(up_all.at[b, yu, :, pl.ds(PART, PART)], by_s.at[i, 0], by_r.at[i, 0], to_yu),
            moved(up_all.at[b, yd, :, pl.ds(PART, PART)], by_s.at[i, 1], by_r.at[i, 1], to_yd),
        ]

    def last_far(i, b, yu, yd, xu, xd):
        lo, hi = pl.ds(0, 2), pl.ds(2, 2)
        return [
            moved(up_all.at[b, lo, xu, pl.ds(0, PART)], ax_s.at[i, 2], ax_r.at[i, 2], to_xu),
            moved(up_all.at[b, hi, xd, pl.ds(0, PART)], ax_s.at[i, 3], ax_r.at[i, 3], to_xd),
            moved(up_all.at[b, yu, lo, pl.ds(PART, PART)], by_s.at[i, 2], by_r.at[i, 2], to_yu),
            moved(up_all.at[b, yd, hi, pl.ds(PART, PART)], by_s.at[i, 3], by_r.at[i, 3], to_yd),
        ]

    own = (y, y, x, x)
    near = (y_down, y_up, x_down, x_up)
    far = (y_far, y_far, x_far, x_far)

    def dx(xu, xd):
        return [moved(down_all.at[z, y, xu], dx_s.at[0], dx_r.at[0], to_xu),
                moved(down_all.at[z, y, xd], dx_s.at[1], dx_r.at[1], to_xd)]

    def dx_far(xu, xd):
        return [moved(down_all.at[z, y, xu, pl.ds(0, 48)], dx_s.at[2], dx_r.at[2], to_xu),
                moved(down_all.at[z, y, xd, pl.ds(48, 48)], dx_s.at[3], dx_r.at[3], to_xd)]

    def dy(yu, yd):
        return [moved(down_all.at[z, yu], dy_s.at[0], dy_r.at[0], to_yu),
                moved(down_all.at[z, yd], dy_s.at[1], dy_r.at[1], to_yd)]

    def dy_far(yu, yd):
        return [moved(down_all.at[z, yu, pl.ds(0, 2)], dy_s.at[2], dy_r.at[2], to_yu),
                moved(down_all.at[z, yd, pl.ds(2, 2)], dy_s.at[3], dy_r.at[3], to_yd)]

    lines = (y, y_down, y_up, y_far)

    def dz(b, i, slot, p, to):
        return moved(down_all.at[b, lines[p]], dz_s.at[i, p], dz_r.at[slot, p], to)

    def start(copies):
        for copy in copies:
            copy.start()

    def landed(copies):
        for copy in copies:
            copy.wait_recv()

    def left(copies):
        for copy in copies:
            copy.wait_send()

    def send_down_line(p):
        dz(z, 1, 1, p, to_zu).start()
        dz(z, 2, 2, p, to_zd).start()

    def pass_up(i):
        b = block(i)

        @pl.when(i < NZ - 1)
        def _():
            landed(uz(i, b, to_zu))

        @pl.when((i < NZ - 3) & (lax.rem(i, 2) == 1))
        def _():
            start(uz(i + 2, b, to_zu))

        @pl.when((i < NZ - 3) & (lax.rem(i, 2) == 0))
        def _():
            start(uz(i + 2, b, to_zd))

        @pl.when(i == NZ - 3)
        def _():
            start(uz_half(i + 2, b, 0, to_zu))

        @pl.when(i == NZ - 2)
        def _():
            start(uz_half(i + 2, b, PART, to_zd))

        @pl.when(i == NZ - 1)
        def _():
            landed(uz_half(i, b, 0, to_zu))
            landed(uz_half(i + 1, b, PART, to_zd))

    def pass_down(s, p):
        for d in (0, 1):
            i = 2 * s - 1 + d
            to = (to_zu, to_zd)[d]
            b = block(i)
            dz(b, i, i, p, to).wait_recv()

            @pl.when(s < 3)
            def _():
                dz(b, i + 2, i + 2, p, to).start()

            if (p < 2) == (d == 0):
                @pl.when(s == 3)
                def _():
                    dz(b, i + 2, NZ - 1, p, to).start()

    def compute(i):
        b = block(i)
        weights = up_all[b].reshape(NY * NX * 2 * PART, 3 * LANES)
        upped[...] = jnp.dot(normed[...], weights, preferred_element_type=jnp.float32)
        taps = taps_all[b]
        lines_of = []
        for yy in range(NY):
            for xx in range(0, NX, 2):
                even, odd = down_all[b, yy, xx], down_all[b, yy, xx + 1]
                half = LANES // 2
                low = jnp.concatenate([even[:, :half], odd[:, :half]], axis=1)
                high = jnp.concatenate([even[:, half:], odd[:, half:]], axis=1)
                lines_of.append(jnp.concatenate([low, high], axis=0))
        down = jnp.concatenate(lines_of, axis=1)
        for part in (0, 1):
            base = part * rows + HALO
            conv = upped[pl.ds(base - 2, rows), :] * taps[0:1]
            conv = conv + upped[pl.ds(base - 1, rows), :] * taps[1:2]
            conv = conv + upped[pl.ds(base, rows), :] * taps[2:3]
            end = conv[:, 2 * LANES :]
            main = jax.nn.gelu(conv[:, LANES : 2 * LANES], approximate=True) * conv[:, :LANES]
            rest = jax.nn.gelu(pltpu.roll(end, LANES // 2, 1), approximate=True) * end
            hidden = jnp.concatenate([main, rest], axis=1).astype(jnp.bfloat16)
            total[part] += jnp.dot(
                hidden[:, : down.shape[0]], down, preferred_element_type=jnp.float32
            )

    start(uz(1, z, to_zu) + uz(2, z, to_zd))
    start(first(0, z, *own))
    start(dx(x, x))
    to_partner = pltpu.make_async_remote_copy(
        src_ref=tokens_ref, dst_ref=rows_all.at[core], send_sem=pair_s, recv_sem=pair_r,
        device_id=to_pair, device_id_type=MESH,
    )
    to_partner.start()
    total[...] = jnp.zeros_like(total)
    pltpu.make_async_remote_copy(
        src_ref=tokens_ref, dst_ref=rows_all.at[1 - core], send_sem=pair_s, recv_sem=pair_r,
        device_id=to_pair, device_id_type=MESH,
    ).wait_recv()
    edge = pltpu.make_async_remote_copy(
        src_ref=rows_all.at[1, pl.ds(rows - HALO, HALO)], dst_ref=halo, send_sem=halo_s,
        recv_sem=halo_r, device_id=to_next, device_id_type=MESH,
    )
    edge.start()

    for i in (1, 2):
        pass_up(jnp.int32(i))
        start(first(i, block(jnp.int32(i)), *own))

    landed(dx(x_down, x_up))
    start(dx_far(x_down, x_up))
    landed(first(0, z, *near))
    start(first_far(0, z, *near))
    scale = norm_in_ref[...]
    for part in (0, 1):
        wide = rows_all[part].astype(jnp.float32)
        normed[pl.ds(HALO + part * rows, rows), :] = normalized(wide, scale).astype(jnp.bfloat16)
    landed(dx_far(x_far, x_far))
    start(dy(y, y))
    send_down_line(0)
    edge.wait_recv()
    origin = (y + x + z) == 0
    before = normalized(halo[...].astype(jnp.float32), scale)
    normed[0:HALO] = jnp.where(origin, 0.0, before).astype(jnp.bfloat16)

    def turn(n, carry):
        @pl.when((n >= 0) & (n + 3 < NZ))
        def _():
            pass_up(n + 3)
            start(first(n + 3, block(n + 3), *own))

        @pl.when(n + 2 < NZ)
        def _():
            landed(first(n + 2, block(n + 2), *near))
            start(first_far(n + 2, block(n + 2), *near))

        @pl.when(n + 1 < NZ)
        def _():
            landed(first_far(n + 1, block(n + 1), *far))
            start(last(n + 1, block(n + 1), *own))

        @pl.when(n == -1)
        def _():
            landed(dy(y_down, y_up))
            start(dy_far(y_down, y_up))
            send_down_line(1)
            send_down_line(2)

        @pl.when(n == 0)
        def _():
            landed(dy_far(y_far, y_far))
            send_down_line(3)

        @pl.when((n >= 1) & (n < NZ - 1))
        def _():
            s = (n + 1) // 2

            @pl.when(lax.rem(n, 2) == 1)
            def _():
                pass_down(s, 0)
                pass_down(s, 1)

            @pl.when(lax.rem(n, 2) == 0)
            def _():
                pass_down(s, 2)
                pass_down(s, 3)

        @pl.when((n >= 0) & (n < NZ))
        def _():
            landed(last(n, block(n), *near))
            start(last_far(n, block(n), *near))

        @pl.when(n == NZ - 1)
        def _():
            for p in range(4):
                dz(block(NZ - 1), NZ - 1 + p // 2, NZ - 1, p, to_zu).wait_recv()

        @pl.when(n >= 1)
        def _():
            landed(last_far(n - 1, block(n - 1), *far))
            compute(n - 1)

        return carry

    lax.fori_loop(-1, NZ + 1, turn, jnp.int32(0))

    pieces = 4
    size = rows // pieces

    def piece(k, ref):
        return pltpu.make_async_remote_copy(
            src_ref=leaving.at[k], dst_ref=ref.at[k], send_sem=sum_s.at[k],
            recv_sem=sum_r.at[k], device_id=to_pair, device_id_type=MESH,
        )

    for k in range(pieces):
        leaving[k] = total[1 - core, pl.ds(k * size, size), :].astype(jnp.bfloat16)
        if k:
            piece(k - 1, arriving).start()
    piece(pieces - 1, arriving).start()
    out_scale = norm_out_ref[...]
    for k in range(pieces):
        piece(k, arriving).wait_recv()
        whole = total[core, pl.ds(k * size, size), :] + arriving[k].astype(jnp.float32)
        out_ref[pl.ds(k * size, size), :] = normalized(whole, out_scale).astype(jnp.bfloat16)

    def drain(i, carry):
        b = block(i)
        left(first(i, b, *own) + first_far(i, b, *near) + last(i, b, *own) + last_far(i, b, *near))
        return carry

    lax.fori_loop(0, NZ, drain, jnp.int32(0))
    for i in range(1, NZ - 1):
        left(uz(i, z, to_zu))
    left(uz_half(NZ - 1, z, 0, to_zu) + uz_half(NZ, z, PART, to_zd))
    left(dx(x, x) + dx_far(x, x) + dy(y, y) + dy_far(y, y))
    for p in range(4):
        for i in range(1, NZ - 1):
            dz(z, i, i, p, to_zu).wait_send()
        dz(z, NZ - 1 + p // 2, NZ - 1, p, to_zu).wait_send()
    to_partner.wait_send()
    edge.wait_send()
    for k in range(pieces):
        piece(k, arriving).wait_send()


def shards(
    tokens, norm_in, value_weight, gate_weight, value_taps, gate_taps, down_weight, norm_out
):
    rows, width = tokens.shape
    bf16, f32 = jnp.bfloat16, jnp.float32
    vmem = pl.BlockSpec(memory_space=pltpu.VMEM)
    return pl.pallas_call(
        kernel,
        in_specs=[vmem] * 8,
        out_specs=vmem,
        out_shape=jax.ShapeDtypeStruct(tokens.shape, tokens.dtype),
        scratch_shapes=[
            pltpu.VMEM((NZ, NY, NX, 2 * PART, 3 * LANES), bf16),
            pltpu.VMEM((NZ, NY, NX, 96, LANES), bf16),
            pltpu.VMEM((NZ, 8, 3 * LANES), f32),
            pltpu.VMEM((2, rows, width), bf16),
            pltpu.VMEM((HALO, width), bf16),
            pltpu.VMEM((2 * rows + HALO, width), bf16),
            pltpu.VMEM((2 * rows + HALO, 3 * LANES), f32),
            pltpu.VMEM((2, rows, width), f32),
            pltpu.VMEM((4, rows // 4, width), bf16),
            pltpu.VMEM((4, rows // 4, width), bf16),
        ]
        + [DMA((NZ + 1,))] * 4
        + [DMA((NZ, 4))] * 8
        + [DMA((4,))] * 4
        + [DMA((NZ + 1, 4)), DMA((NZ, 4))]
        + [DMA] * 4
        + [DMA((4,))] * 2,
        compiler_params=pltpu.CompilerParams(
            collective_id=0, has_side_effects=True, vmem_limit_bytes=56 * 2**20
        ),
    )(
        tokens, norm_in[None], value_weight, gate_weight, value_taps, gate_taps, down_weight,
        norm_out[None],
    )


def solution(mesh):
    split = Mesh(mesh.devices.reshape(NY, NX, NZ, 2), ALL)
    return jax.shard_map(
        shards,
        mesh=split,
        in_specs=(
            P(ALL, None),
            P(),
            P(FS, ("z", "core")),
            P(FS, ("z", "core")),
            P(None, ("z", "core")),
            P(None, ("z", "core")),
            P(("z", "core"), FS),
            P(),
        ),
        out_specs=P(ALL, None),
        check_vma=False,
    )
```

time: 277 us -> 69.5 us (0.25)
  waiting for transfers between devices: 202 us -> 0 us
  Pallas kernels: 13.4 us -> 65.9 us
  blocking collectives: 23.4 us -> 0 us
  between operations: 13.5 us -> 0.01 us
  starting transfers between devices: 12.6 us -> 0 us
  local copies, waits for them, and re-layouts: 8.07 us -> 3.35 us
  other arithmetic: 3.41 us -> 0 us
    all_gather x2 -> x0, waiting for transfers between devices: 198 us -> none  [the longest x1 121 us: shards(): up_all = lax.all_gather(up, GATHER)]
    pallas_call x1, Pallas kernels: 13.4 us -> 65.9 us  [shards(): pl.pallas_call(kernel, in_specs=[vmem] * 8, out_specs=vmem, out_shape=jax...]
    all_gather x1 -> x0, blocking collectives: 23.4 us -> none  [shards(): taps_all = lax.all_gather(taps, 'z')]
    ppermute x5 -> x0, starting transfers between devices: 12.6 us -> none  [the longest x4 10.7 us: swapped(): lax.ppermute(value, axis, [(i, i ^ 1) for i in range(lax.axis_size(axis))])]
    slice x9 -> x0, local copies, waits for them, and re-layouts: 6.37 us -> none  [the longest x2 1.4 us: packed_up(): value[:, LANES:]]
    ppermute x5 -> x0, waiting for transfers between devices: 4.15 us -> none  [the longest x4 2.98 us: swapped(): lax.ppermute(value, axis, [(i, i ^ 1) for i in range(lax.axis_size(axis))])]
  transfers between devices with their start and end apart: 7 -> 0, of which waited for: 5 -> 0; matrix products, arithmetic and copies ran while one was open for 3% -> 0% of each run, Pallas kernels for 0% -> 0%
where the time goes in v2:
time: 69.5 us; the launch traced here: 69.3 us
  Pallas kernels  65.9 us (95%)
  local copies, waits for them, and re-layouts  3.35 us (5%)
    pallas_call x1, Pallas kernels, shards(): pl.pallas_call(kernel, in_specs=[vmem] * 8, out_specs=vmem, out_shape=jax...  65.9 us
    unnamed x2, local copies, waits for them, and re-layouts  3.35 us

profile of v2, /device:TPU:1, one launch (start us, length us, event | category | flops | bytes accessed | tf_op | source)
XLA Modules:
  0.0 69.3 jit_solution(12506094544071217561)
XLA Ops:
  0.0 1.5 %copy.9.down_ref = bf16[176,64]{1,0:T(8,128)(2,1)} copy(bf16[176,64]{0,1:T(8,128)(2,1)} %param.14) | data formatting | bytes 45056 | tf_op args[6]
  1.5 65.9 %shard_map.82 = bf16[256,1024]{1,0:T(8,128)(2,1)} custom-call(bf16[256,1024]{1,0:T(8,128)(2,1)} %tokens_ref.1, f32[1,1024]{1,0:T(1,128)} %bitcast.2, bf16[64,176]{1,0:T(8,128)(2,1)} %value_ref.1, bf16[64,176]{1,0:T(8,128)(2,1)} %gate_ref.1, f32[3,176]{1,0:T(4,128)} %value_taps_ref.1, f32[3,176]{1,0:T(4,128)} %gate_taps_ref.1, bf16[176,64]{1,0:T(8,128)(2,1)} %copy.9.down_ref, ...), custom_call_target="tpu_custom_call" | custom-call | tf_op jit(solution)/shard_map/pallas_call | solution.py:406
  67.4 1.9 %copy.11 = bf16[256,1024]{1,0:T(8,128)(2,1)} copy(bf16[256,1024]{1,0:T(8,128)(2,1)} %shard_map.82) | data formatting | bytes 1048576

commit v3 on v2

v3 whole, which is shorter than its diff:
```python
import jax
import jax.numpy as jnp
from jax import lax
from jax.experimental import pallas as pl
from jax.experimental.pallas import tpu as pltpu
from jax.sharding import Mesh
from jax.sharding import PartitionSpec as P

FS = ("y", "x")
ALL = ("y", "x", "z", "core")
MESH = pl.DeviceIdType.MESH
DMA = pltpu.SemaphoreType.DMA

norm_eps = 1e-06
HALO = 16
LANES = 128
NX = NY = 4
NZ = 8
PART = 32


def packed_up(value, gate):
    tail = value.shape[1] - LANES
    pad = jnp.zeros((value.shape[0], LANES // 2 - tail), value.dtype)
    return jnp.concatenate(
        [value[:, :LANES], gate[:, :LANES], value[:, LANES:], pad, gate[:, LANES:], pad],
        axis=1,
    )


def packed_down(down):
    half = 96
    pad = jnp.zeros((2 * half - down.shape[0], down.shape[1]), down.dtype)
    low = jnp.concatenate([down[half:], pad], axis=0)
    return jnp.concatenate([down[:half], low], axis=1)


def normalized(wide, scale):
    power = jnp.mean(wide * wide, axis=-1, keepdims=True)
    return wide * lax.rsqrt(power + norm_eps) * scale


def moved(ref, send, recv, to):
    return pltpu.make_async_remote_copy(
        src_ref=ref, dst_ref=ref, send_sem=send, recv_sem=recv, device_id=to, device_id_type=MESH
    )


def start(*copies):
    for copy in copies:
        copy.start()


def kernel(
    tokens_ref,
    norm_in_ref,
    value_ref,
    gate_ref,
    value_taps_ref,
    gate_taps_ref,
    down_ref,
    norm_out_ref,
    out_ref,
    value_in,
    gate_in,
    down_in,
    up_all,
    down_all,
    taps_all,
    rows_all,
    halo,
    normed,
    upped,
    total,
    leaving,
    arriving,
    first_s, last_s, uz_s, dxy_s, dz_s,
    uz_r, near_r, far_r, last_r, last_far_r, dx_r, dy_r, dz_r,
    load_s, pair_s, pair_r, halo_s, halo_r, sum_s, sum_r,
):
    y, x, z, core = (lax.axis_index(name) for name in ALL)
    rows = out_ref.shape[0]
    x_up, x_down, x_far = (lax.rem(x + k, NX) for k in (1, 3, 2))
    y_up, y_down, y_far = (lax.rem(y + k, NY) for k in (1, 3, 2))
    z_up, z_down = lax.rem(z + 1, NZ), lax.rem(z + NZ - 1, NZ)
    to_xu, to_xd = {"x": x_up}, {"x": x_down}
    to_yu, to_yd = {"y": y_up}, {"y": y_down}
    to_zu, to_zd = {"z": z_up}, {"z": z_down}
    to_pair = {"core": 1 - core}
    z_wrap = (z + 1) // NZ
    x_wrap = (x + z_wrap) // NX
    to_next = {"z": z_up, "x": lax.rem(x + z_wrap, NX), "y": lax.rem(y + x_wrap, NY)}
    z_back = 1 - (z + NZ - 1) // NZ
    x_back = 1 - (x + NX - z_back) // NX
    to_prev = {"z": z_down, "x": lax.rem(x + NX - z_back, NX), "y": lax.rem(y + NY - x_back, NY)}

    barrier = pltpu.get_barrier_semaphore()
    for device in (to_xu, to_xd, to_yu, to_yd, to_zu, to_zd, to_pair, to_prev):
        pl.semaphore_signal(barrier, inc=1, device_id=device, device_id_type=MESH)
    loads = [
        pltpu.make_async_copy(value_ref, value_in, load_s.at[0]),
        pltpu.make_async_copy(gate_ref, gate_in, load_s.at[1]),
        pltpu.make_async_copy(down_ref, down_in, load_s.at[2]),
        pltpu.make_async_copy(tokens_ref, rows_all.at[core], load_s.at[3]),
    ]
    for load in loads:
        load.start()
    taps_all[z, 0:3] = packed_up(value_taps_ref[...], gate_taps_ref[...])
    total[...] = jnp.zeros_like(total)
    for load in loads:
        load.wait()
    up_all[z, y, x] = packed_up(value_in[...], gate_in[...])
    down_all[z, y, x] = packed_down(down_in[...].T)
    pl.semaphore_wait(barrier, 8)

    def block(i):
        step = (i + 1) // 2
        return lax.rem(z + NZ + step - 2 * step * lax.rem(i, 2), NZ)

    lines = (y, y_down, y_up, y_far)
    posts = (x, x_down, x_up, x_far)
    upper, lower = pl.ds(0, PART), pl.ds(PART, PART)

    def landed(ref, sem):
        moved(ref, pair_s, sem, to_pair).wait_recv()

    def left(ref, sem):
        moved(ref, sem, pair_r, to_pair).wait_send()

    def uz(i, b, to):
        start(
            moved(up_all.at[b, y, x], uz_s, uz_r.at[i - 1], to),
            moved(taps_all.at[b], uz_s, uz_r.at[i - 1], to),
        )

    def pass_up(i):
        b = block(i)
        landed(upped.at[pl.ds(0, 40)], uz_r.at[i - 1])

        @pl.when((i < NZ - 3) & (lax.rem(i, 2) == 1))
        def _():
            uz(i + 2, b, to_zu)

        @pl.when((i < NZ - 3) & (lax.rem(i, 2) == 0))
        def _():
            uz(i + 2, b, to_zd)

        @pl.when(i == NZ - 3)
        def _():
            start(
                moved(up_all.at[b, y, x, upper], uz_s, uz_r.at[NZ - 2], to_zu),
                moved(taps_all.at[b], uz_s, uz_r.at[NZ - 2], to_zu),
            )

        @pl.when(i == NZ - 2)
        def _():
            start(moved(up_all.at[b, y, x, lower], uz_s, uz_r.at[NZ - 2], to_zd))

    def first(i, b):
        near = near_r.at[i]
        start(
            moved(up_all.at[b, y, x, upper], first_s, near, to_yu),
            moved(up_all.at[b, y, x, upper], first_s, near, to_yd),
            moved(up_all.at[b, y, x, lower], first_s, near, to_xu),
            moved(up_all.at[b, y, x, lower], first_s, near, to_xd),
        )

    def relay(i, b):
        h = PART // 2
        far = far_r.at[i]
        landed(up_all.at[b, y, pl.ds(0, 2)], near_r.at[i])
        start(
            moved(up_all.at[b, y_down, x, pl.ds(0, h)], first_s, far, to_yu),
            moved(up_all.at[b, y_up, x, pl.ds(h, h)], first_s, far, to_yd),
            moved(up_all.at[b, y, x_down, pl.ds(PART, h)], first_s, far, to_xu),
            moved(up_all.at[b, y, x_up, pl.ds(PART + h, h)], first_s, far, to_xd),
        )

    def last(i, b, p):
        there = last_r.at[i, (p + 1) // 2]
        start(
            moved(up_all.at[b, lines[p], x, upper], last_s, there, to_xu),
            moved(up_all.at[b, y, posts[p], lower], last_s, there, to_yu),
            moved(up_all.at[b, lines[p], x, upper], last_s, there, to_xd),
            moved(up_all.at[b, y, posts[p], lower], last_s, there, to_yd),
        )

    def finish(i, b):
        landed(up_all.at[b, y, x], far_r.at[i])
        for p in (1, 2, 3):
            last(i, b, p)

    def hand_on(i, b, *ps):
        landed(up_all.at[b, y, pl.ds(0, 2 * len(ps))], last_r.at[i, (ps[0] + 1) // 2])
        there = last_far_r.at[i]
        for p in ps:
            px, to_x, py, to_y = (
                (x_down, to_xu, y_down, to_yu) if p < 2 else (x_up, to_xd, y_up, to_yd)
            )
            start(
                moved(up_all.at[b, lines[p], px, upper], last_s, there, to_x),
                moved(up_all.at[b, py, posts[p], lower], last_s, there, to_y),
            )

    def complete(i, b):
        landed(up_all.at[b, 0], last_far_r.at[i])

    def send_down_line(p):
        start(
            moved(down_all.at[z, lines[p]], dz_s, dz_r.at[0, p], to_zu),
            moved(down_all.at[z, lines[p]], dz_s, dz_r.at[0, p], to_zd),
        )

    def pass_down(s, p):
        landed(down_all.at[0, pl.ds(0, 2)], dz_r.at[s - 1, p])
        for d in (0, 1):
            b, to = block(2 * s - 1 + d), (to_zu, to_zd)[d]

            @pl.when(s < 3)
            def _():
                moved(down_all.at[b, lines[p]], dz_s, dz_r.at[s, p], to).start()

            if (p < 2) == (d == 0):
                @pl.when(s == 3)
                def _():
                    moved(down_all.at[b, lines[p]], dz_s, dz_r.at[3, 0], to).start()

    def compute(i):
        b = block(i)
        weights = up_all[b].reshape(NY * NX * 2 * PART, 3 * LANES)
        upped[...] = jnp.dot(normed[...], weights, preferred_element_type=jnp.float32)
        taps = taps_all[b]
        lines_of = []
        for yy in range(NY):
            for xx in range(0, NX, 2):
                even, odd = down_all[b, yy, xx], down_all[b, yy, xx + 1]
                half = LANES // 2
                low = jnp.concatenate([even[:, :half], odd[:, :half]], axis=1)
                high = jnp.concatenate([even[:, half:], odd[:, half:]], axis=1)
                lines_of.append(jnp.concatenate([low, high], axis=0))
        down = jnp.concatenate(lines_of, axis=1)
        for part in (0, 1):
            base = part * rows + HALO
            conv = upped[pl.ds(base - 2, rows), :] * taps[0:1]
            conv = conv + upped[pl.ds(base - 1, rows), :] * taps[1:2]
            conv = conv + upped[pl.ds(base, rows), :] * taps[2:3]
            end = conv[:, 2 * LANES :]
            main = jax.nn.gelu(conv[:, LANES : 2 * LANES], approximate=True) * conv[:, :LANES]
            rest = jax.nn.gelu(pltpu.roll(end, LANES // 2, 1), approximate=True) * end
            hidden = jnp.concatenate([main, rest], axis=1).astype(jnp.bfloat16)
            total[part] += jnp.dot(
                hidden[:, : down.shape[0]], down, preferred_element_type=jnp.float32
            )

    def at(i):
        return jnp.int32(i), block(jnp.int32(i))

    uz(1, z, to_zu)
    uz(2, z, to_zd)
    dx_near, dx_far = dx_r.at[0], dx_r.at[1]
    start(
        moved(down_all.at[z, y, x], dxy_s, dx_near, to_xu),
        moved(down_all.at[z, y, x], dxy_s, dx_near, to_xd),
    )
    first(*at(0))
    own_rows = moved(rows_all.at[core], pair_s, pair_r, to_pair)
    own_rows.start()

    landed(down_all.at[z, y, pl.ds(0, 2)], dx_near)
    start(
        moved(down_all.at[z, y, x_down, pl.ds(0, 48)], dxy_s, dx_far, to_xu),
        moved(down_all.at[z, y, x_up, pl.ds(48, 48)], dxy_s, dx_far, to_xd),
    )
    relay(*at(0))
    last(*at(0), 0)
    landed(rows_all.at[1 - core], pair_r)
    edge = pltpu.make_async_remote_copy(
        src_ref=rows_all.at[1, pl.ds(rows - HALO, HALO)], dst_ref=halo, send_sem=halo_s,
        recv_sem=halo_r, device_id=to_next, device_id_type=MESH,
    )
    edge.start()
    for i in (1, 2):
        pass_up(jnp.int32(i))
        first(*at(i))

    landed(down_all.at[z, y, x], dx_far)
    dy_near, dy_far = dy_r.at[0], dy_r.at[1]
    start(
        moved(down_all.at[z, y], dxy_s, dy_near, to_yu),
        moved(down_all.at[z, y], dxy_s, dy_near, to_yd),
    )
    send_down_line(0)
    finish(*at(0))
    hand_on(*at(0), 0)
    for i in (1, 2):
        relay(*at(i))
        last(*at(i), 0)
    scale = norm_in_ref[...]
    for part in (0, 1):
        wide = rows_all[part].astype(jnp.float32)
        normed[pl.ds(HALO + part * rows, rows), :] = normalized(wide, scale).astype(jnp.bfloat16)
    for i in (3, 4):
        pass_up(jnp.int32(i))
        first(*at(i))
    landed(down_all.at[z, pl.ds(0, 2)], dy_near)
    start(
        moved(down_all.at[z, y_down, pl.ds(0, 2)], dxy_s, dy_far, to_yu),
        moved(down_all.at[z, y_up, pl.ds(2, 2)], dxy_s, dy_far, to_yd),
    )
    send_down_line(1)
    send_down_line(2)
    finish(*at(1))
    hand_on(*at(0), 1, 2)
    edge.wait_recv()
    origin = (y + x + z) == 0
    before = normalized(halo[...].astype(jnp.float32), scale)
    normed[0:HALO] = jnp.where(origin, 0.0, before).astype(jnp.bfloat16)

    def turn(n, carry):
        @pl.when(n + 5 < NZ)
        def _():
            pass_up(n + 5)
            first(n + 5, block(n + 5))

        @pl.when(n + 3 < NZ)
        def _():
            relay(n + 3, block(n + 3))
            last(n + 3, block(n + 3), 0)

        @pl.when(n == 0)
        def _():
            landed(down_all.at[z, 0], dy_far)
            send_down_line(3)

        @pl.when(n + 2 < NZ)
        def _():
            finish(n + 2, block(n + 2))

        @pl.when(n + 1 < NZ)
        def _():
            hand_on(n + 1, block(n + 1), 0)
            hand_on(n + 1, block(n + 1), 1, 2)

        hand_on(n, block(n), 3)

        @pl.when(n < NZ - 2)
        def _():
            s = (n + 2) // 2

            @pl.when(lax.rem(n, 2) == 0)
            def _():
                pass_down(s, 0)
                pass_down(s, 1)

            @pl.when(lax.rem(n, 2) == 1)
            def _():
                pass_down(s, 2)
                pass_down(s, 3)

        @pl.when(n == NZ - 1)
        def _():
            landed(down_all.at[0], dz_r.at[3, 0])

        complete(n, block(n))
        compute(n)
        return carry

    lax.fori_loop(0, NZ, turn, jnp.int32(0))

    pieces = 4
    size = rows // pieces

    def piece(k, ref):
        return pltpu.make_async_remote_copy(
            src_ref=leaving.at[k], dst_ref=ref.at[k], send_sem=sum_s,
            recv_sem=sum_r.at[k], device_id=to_pair, device_id_type=MESH,
        )

    for k in range(pieces):
        leaving[k] = total[1 - core, pl.ds(k * size, size), :].astype(jnp.bfloat16)
        if k:
            piece(k - 1, arriving).start()
    piece(pieces - 1, arriving).start()
    out_scale = norm_out_ref[...]
    for k in range(pieces):
        piece(k, arriving).wait_recv()
        whole = total[core, pl.ds(k * size, size), :] + arriving[k].astype(jnp.float32)
        out_ref[pl.ds(k * size, size), :] = normalized(whole, out_scale).astype(jnp.bfloat16)

    left(up_all.at[pl.ds(0, 6), 0], first_s)
    left(up_all.at[pl.ds(0, 6)], last_s)
    left(upped.at[pl.ds(0, 280)], uz_s)
    left(down_all.at[pl.ds(0, 5), 0, pl.ds(0, 3)], dxy_s)
    left(down_all.at[pl.ds(0, 7)], dz_s)
    own_rows.wait_send()
    edge.wait_send()
    left(leaving, sum_s)


def shards(
    tokens, norm_in, value_weight, gate_weight, value_taps, gate_taps, down_weight, norm_out
):
    rows, width = tokens.shape
    bf16, f32 = jnp.bfloat16, jnp.float32
    vmem = pl.BlockSpec(memory_space=pltpu.VMEM)
    hbm = pl.BlockSpec(memory_space=pl.ANY)
    return pl.pallas_call(
        kernel,
        in_specs=[hbm, vmem, hbm, hbm, vmem, vmem, hbm, vmem],
        out_specs=vmem,
        out_shape=jax.ShapeDtypeStruct(tokens.shape, tokens.dtype),
        scratch_shapes=[
            pltpu.VMEM(value_weight.shape, bf16),
            pltpu.VMEM(value_weight.shape, bf16),
            pltpu.VMEM(down_weight.shape[::-1], bf16),
            pltpu.VMEM((NZ, NY, NX, 2 * PART, 3 * LANES), bf16),
            pltpu.VMEM((NZ, NY, NX, 96, LANES), bf16),
            pltpu.VMEM((NZ, 8, 3 * LANES), f32),
            pltpu.VMEM((2, rows, width), bf16),
            pltpu.VMEM((HALO, width), bf16),
            pltpu.VMEM((2 * rows + HALO, width), bf16),
            pltpu.VMEM((2 * rows + HALO, 3 * LANES), f32),
            pltpu.VMEM((2, rows, width), f32),
            pltpu.VMEM((4, rows // 4, width), bf16),
            pltpu.VMEM((4, rows // 4, width), bf16),
        ]
        + [DMA] * 5
        + [DMA((NZ - 1,))]
        + [DMA((NZ,))] * 2
        + [DMA((NZ, 3)), DMA((NZ,))]
        + [DMA((2,))] * 2
        + [DMA((4, 4)), DMA((4,))]
        + [DMA] * 5
        + [DMA((4,))],
        compiler_params=pltpu.CompilerParams(
            collective_id=0, has_side_effects=True, vmem_limit_bytes=56 * 2**20
        ),
    )(
        tokens, norm_in[None], value_weight, gate_weight, value_taps, gate_taps, down_weight.T,
        norm_out[None],
    )


def solution(mesh):
    split = Mesh(mesh.devices.reshape(NY, NX, NZ, 2), ALL)
    return jax.shard_map(
        shards,
        mesh=split,
        in_specs=(
            P(ALL, None),
            P(),
            P(FS, ("z", "core")),
            P(FS, ("z", "core")),
            P(None, ("z", "core")),
            P(None, ("z", "core")),
            P(("z", "core"), FS),
            P(),
        ),
        out_specs=P(ALL, None),
        check_vma=False,
    )
```

time: 69.5 us -> 81.8 us (1.18)
  Pallas kernels: 65.9 us -> 79.8 us
  local copies, waits for them, and re-layouts: 3.35 us -> 1.87 us
    pallas_call x1, Pallas kernels: 65.9 us -> 79.8 us  [shards(): pl.pallas_call(kernel, in_specs=[hbm, vmem, hbm, hbm, vmem, vmem, hbm, vm...]
    unnamed x2 -> x1, local copies, waits for them, and re-layouts: 3.35 us -> 1.87 us
where the time goes in v3:
time: 81.8 us; the launch traced here: 81.6 us
  Pallas kernels  79.8 us (98%)
  local copies, waits for them, and re-layouts  1.87 us (2%)
    pallas_call x1, Pallas kernels, shards(): pl.pallas_call(kernel, in_specs=[hbm, vmem, hbm, hbm, vmem, vmem, hbm, vm...  79.8 us
    unnamed x1, local copies, waits for them, and re-layouts  1.87 us

profile of v3, /device:TPU:1, one launch (start us, length us, event | category | flops | bytes accessed | tf_op | source)
XLA Modules:
  0.0 81.6 jit_solution(17947257661940117789)
XLA Ops:
  0.0 79.8 %shard_map.82 = bf16[256,1024]{1,0:T(8,128)(2,1)} custom-call(bf16[256,1024]{1,0:T(8,128)(2,1)} %tokens_ref.1, f32[1,1024]{1,0:T(1,128)} %bitcast.4, bf16[64,176]{1,0:T(8,128)(2,1)} %value_ref.1, bf16[64,176]{1,0:T(8,128)(2,1)} %gate_ref.1, f32[3,176]{1,0:T(4,128)} %value_taps_ref.1, f32[3,176]{1,0:T(4,128)} %gate_taps_ref.1, bf16[64,176]{1,0:T(8,128)(2,1)} %bitcast.3, ...), custom_call_target="tpu_custom_call" | custom-call | tf_op jit(solution)/shard_map/pallas_call | solution.py:407
  79.8 1.9 %copy.10 = bf16[256,1024]{1,0:T(8,128)(2,1)} copy(bf16[256,1024]{1,0:T(8,128)(2,1)} %shard_map.82) | data formatting | bytes 1048576

commit v4 on v3

--- a/solution.py
+++ b/solution.py
@@ -252,9 +252,6 @@
                 hidden[:, : down.shape[0]], down, preferred_element_type=jnp.float32
             )
 
-    def at(i):
-        return jnp.int32(i), block(jnp.int32(i))
-
     uz(1, z, to_zu)
     uz(2, z, to_zd)
     dx_near, dx_far = dx_r.at[0], dx_r.at[1]
@@ -262,88 +259,100 @@
         moved(down_all.at[z, y, x], dxy_s, dx_near, to_xu),
         moved(down_all.at[z, y, x], dxy_s, dx_near, to_xd),
     )
-    first(*at(0))
+    first(jnp.int32(0), z)
     own_rows = moved(rows_all.at[core], pair_s, pair_r, to_pair)
     own_rows.start()
-
-    landed(down_all.at[z, y, pl.ds(0, 2)], dx_near)
-    start(
-        moved(down_all.at[z, y, x_down, pl.ds(0, 48)], dxy_s, dx_far, to_xu),
-        moved(down_all.at[z, y, x_up, pl.ds(48, 48)], dxy_s, dx_far, to_xd),
-    )
-    relay(*at(0))
-    last(*at(0), 0)
-    landed(rows_all.at[1 - core], pair_r)
     edge = pltpu.make_async_remote_copy(
         src_ref=rows_all.at[1, pl.ds(rows - HALO, HALO)], dst_ref=halo, send_sem=halo_s,
         recv_sem=halo_r, device_id=to_next, device_id_type=MESH,
     )
-    edge.start()
-    for i in (1, 2):
-        pass_up(jnp.int32(i))
-        first(*at(i))
-
-    landed(down_all.at[z, y, x], dx_far)
     dy_near, dy_far = dy_r.at[0], dy_r.at[1]
-    start(
-        moved(down_all.at[z, y], dxy_s, dy_near, to_yu),
-        moved(down_all.at[z, y], dxy_s, dy_near, to_yd),
-    )
-    send_down_line(0)
-    finish(*at(0))
-    hand_on(*at(0), 0)
-    for i in (1, 2):
-        relay(*at(i))
-        last(*at(i), 0)
-    scale = norm_in_ref[...]
-    for part in (0, 1):
-        wide = rows_all[part].astype(jnp.float32)
-        normed[pl.ds(HALO + part * rows, rows), :] = normalized(wide, scale).astype(jnp.bfloat16)
-    for i in (3, 4):
-        pass_up(jnp.int32(i))
-        first(*at(i))
-    landed(down_all.at[z, pl.ds(0, 2)], dy_near)
-    start(
-        moved(down_all.at[z, y_down, pl.ds(0, 2)], dxy_s, dy_far, to_yu),
-        moved(down_all.at[z, y_up, pl.ds(2, 2)], dxy_s, dy_far, to_yd),
-    )
-    send_down_line(1)
-    send_down_line(2)
-    finish(*at(1))
-    hand_on(*at(0), 1, 2)
-    edge.wait_recv()
-    origin = (y + x + z) == 0
-    before = normalized(halo[...].astype(jnp.float32), scale)
-    normed[0:HALO] = jnp.where(origin, 0.0, before).astype(jnp.bfloat16)
+
+    def normalize_rows():
+        scale = norm_in_ref[...]
+        for part in (0, 1):
+            wide = rows_all[part].astype(jnp.float32)
+            value = normalized(wide, scale).astype(jnp.bfloat16)
+            normed[pl.ds(HALO + part * rows, rows), :] = value
+
+    def normalize_halo():
+        edge.wait_recv()
+        origin = (y + x + z) == 0
+        before = normalized(halo[...].astype(jnp.float32), norm_in_ref[...])
+        normed[0:HALO] = jnp.where(origin, 0.0, before).astype(jnp.bfloat16)
 
     def turn(n, carry):
-        @pl.when(n + 5 < NZ)
-        def _():
+        @pl.when(n == -4)
+        def _():
+            landed(down_all.at[z, y, pl.ds(0, 2)], dx_near)
+            start(
+                moved(down_all.at[z, y, x_down, pl.ds(0, 48)], dxy_s, dx_far, to_xu),
+                moved(down_all.at[z, y, x_up, pl.ds(48, 48)], dxy_s, dx_far, to_xd),
+            )
             pass_up(n + 5)
             first(n + 5, block(n + 5))
 
-        @pl.when(n + 3 < NZ)
-        def _():
-            relay(n + 3, block(n + 3))
-            last(n + 3, block(n + 3), 0)
-
-        @pl.when(n == 0)
+        @pl.when(n == -3)
+        def _():
+            landed(down_all.at[z, y, x], dx_far)
+            start(
+                moved(down_all.at[z, y], dxy_s, dy_near, to_yu),
+                moved(down_all.at[z, y], dxy_s, dy_near, to_yd),
+            )
+            send_down_line(0)
+
+        @pl.when(n == -2)
+        def _():
+            landed(down_all.at[z, pl.ds(0, 2)], dy_near)
+            start(
+                moved(down_all.at[z, y_down, pl.ds(0, 2)], dxy_s, dy_far, to_yu),
+                moved(down_all.at[z, y_up, pl.ds(2, 2)], dxy_s, dy_far, to_yd),
+            )
+            send_down_line(1)
+            send_down_line(2)
+
+        @pl.when(n == -1)
         def _():
             landed(down_all.at[z, 0], dy_far)
             send_down_line(3)
 
-        @pl.when(n + 2 < NZ)
-        def _():
-            finish(n + 2, block(n + 2))
-
-        @pl.when(n + 1 < NZ)
-        def _():
-            hand_on(n + 1, block(n + 1), 0)
+        @pl.when(n + 6 < NZ)
+        def _():
+            pass_up(n + 6)
+            first(n + 6, block(n + 6))
+
+        @pl.when(n + 4 < NZ)
+        def _():
+            relay(n + 4, block(n + 4))
+
+        @pl.when((n >= -1) & (n + 1 < NZ))
+        def _():
             hand_on(n + 1, block(n + 1), 1, 2)
-
-        hand_on(n, block(n), 3)
-
-        @pl.when(n < NZ - 2)
+            hand_on(n + 1, block(n + 1), 3)
+
+        @pl.when((n >= -2) & (n + 2 < NZ))
+        def _():
+            hand_on(n + 2, block(n + 2), 0)
+
+        @pl.when((n >= -3) & (n + 3 < NZ))
+        def _():
+            finish(n + 3, block(n + 3))
+
+        @pl.when(n + 4 < NZ)
+        def _():
+            last(n + 4, block(n + 4), 0)
+
+        @pl.when(n == -4)
+        def _():
+            landed(rows_all.at[1 - core], pair_r)
+            edge.start()
+            normalize_rows()
+
+        @pl.when(n == -1)
+        def _():
+            normalize_halo()
+
+        @pl.when((n >= 0) & (n < NZ - 2))
         def _():
             s = (n + 2) // 2
 
@@ -361,11 +370,14 @@
         def _():
             landed(down_all.at[0], dz_r.at[3, 0])
 
-        complete(n, block(n))
-        compute(n)
+        @pl.when(n >= 0)
+        def _():
+            complete(n, block(n))
+            compute(n)
+
         return carry
 
-    lax.fori_loop(0, NZ, turn, jnp.int32(0))
+    lax.fori_loop(-4, NZ, turn, jnp.int32(0))
 
     pieces = 4
     size = rows // pieces

time: 81.8 us -> 61.7 us (0.75)
  Pallas kernels: 79.8 us -> 59.7 us
    pallas_call x1, Pallas kernels: 79.8 us -> 59.7 us  [shards(): pl.pallas_call(kernel, in_specs=[hbm, vmem, hbm, hbm, vmem, vmem, hbm, vm...]
where the time goes in v4:
time: 61.7 us; the launch traced here: 61.5 us
  Pallas kernels  59.7 us (97%)
  local copies, waits for them, and re-layouts  1.87 us (3%)
    pallas_call x1, Pallas kernels, shards(): pl.pallas_call(kernel, in_specs=[hbm, vmem, hbm, hbm, vmem, vmem, hbm, vm...  59.7 us
    unnamed x1, local copies, waits for them, and re-layouts  1.87 us

profile of v4, /device:TPU:1, one launch (start us, length us, event | category | flops | bytes accessed | tf_op | source)
XLA Modules:
  0.0 61.5 jit_solution(16898367140498671064)
XLA Ops:
  0.0 59.7 %shard_map.82 = bf16[256,1024]{1,0:T(8,128)(2,1)} custom-call(bf16[256,1024]{1,0:T(8,128)(2,1)} %tokens_ref.1, f32[1,1024]{1,0:T(1,128)} %bitcast.4, bf16[64,176]{1,0:T(8,128)(2,1)} %value_ref.1, bf16[64,176]{1,0:T(8,128)(2,1)} %gate_ref.1, f32[3,176]{1,0:T(4,128)} %value_taps_ref.1, f32[3,176]{1,0:T(4,128)} %gate_taps_ref.1, bf16[64,176]{1,0:T(8,128)(2,1)} %bitcast.3, ...), custom_call_target="tpu_custom_call" | custom-call | tf_op jit(solution)/shard_map/pallas_call | solution.py:419
  59.7 1.9 %copy.10 = bf16[256,1024]{1,0:T(8,128)(2,1)} copy(bf16[256,1024]{1,0:T(8,128)(2,1)} %shard_map.82) | data formatting | bytes 1048576

commit v5 on v4

--- a/solution.py
+++ b/solution.py
@@ -187,8 +187,7 @@
 
     def finish(i, b):
         landed(up_all.at[b, y, x], far_r.at[i])
-        for p in (1, 2, 3):
-            last(i, b, p)
+        last(i, b, 3)
 
     def hand_on(i, b, *ps):
         landed(up_all.at[b, y, pl.ds(0, 2 * len(ps))], last_r.at[i, (ps[0] + 1) // 2])
@@ -205,11 +204,41 @@
     def complete(i, b):
         landed(up_all.at[b, 0], last_far_r.at[i])
 
-    def send_down_line(p):
-        start(
-            moved(down_all.at[z, lines[p]], dz_s, dz_r.at[0, p], to_zu),
-            moved(down_all.at[z, lines[p]], dz_s, dz_r.at[0, p], to_zd),
-        )
+    def down_x():
+        start(
+            moved(down_all.at[z, y, x], dxy_s, dx_r.at[0], to_xu),
+            moved(down_all.at[z, y, x], dxy_s, dx_r.at[0], to_xd),
+        )
+
+    def down_x_far():
+        start(
+            moved(down_all.at[z, y, x_down, pl.ds(0, 48)], dxy_s, dx_r.at[1], to_xu),
+            moved(down_all.at[z, y, x_up, pl.ds(48, 48)], dxy_s, dx_r.at[1], to_xd),
+        )
+
+    def down_y(c):
+        there = dy_r.at[(c + 1) // 2]
+        start(
+            moved(down_all.at[z, y, posts[c]], dxy_s, there, to_yu),
+            moved(down_all.at[z, y, posts[c]], dxy_s, there, to_yd),
+        )
+
+    def down_y_far(c):
+        there = dy_r.at[3 + (c + 1) // 2]
+        start(
+            moved(down_all.at[z, y_down, posts[c], pl.ds(0, 48)], dxy_s, there, to_yu),
+            moved(down_all.at[z, y_up, posts[c], pl.ds(48, 48)], dxy_s, there, to_yd),
+        )
+
+    def down_z(p, *cs):
+        for c in cs:
+            start(
+                moved(down_all.at[z, lines[p], posts[c]], dz_s, dz_r.at[0, p], to_zu),
+                moved(down_all.at[z, lines[p], posts[c]], dz_s, dz_r.at[0, p], to_zd),
+            )
+
+    def down_landed(count, sem):
+        landed(down_all.at[z, 0, pl.ds(0, count)], sem)
 
     def pass_down(s, p):
         landed(down_all.at[0, pl.ds(0, 2)], dz_r.at[s - 1, p])
@@ -225,48 +254,55 @@
                 def _():
                     moved(down_all.at[b, lines[p]], dz_s, dz_r.at[3, 0], to).start()
 
-    def compute(i):
-        b = block(i)
+    def project(b, lo, count):
         weights = up_all[b].reshape(NY * NX * 2 * PART, 3 * LANES)
-        upped[...] = jnp.dot(normed[...], weights, preferred_element_type=jnp.float32)
-        taps = taps_all[b]
+        upped[lo : lo + count] = jnp.dot(
+            normed[lo : lo + count], weights, preferred_element_type=jnp.float32
+        )
+
+    def down_of(b):
+        half = LANES // 2
         lines_of = []
         for yy in range(NY):
             for xx in range(0, NX, 2):
                 even, odd = down_all[b, yy, xx], down_all[b, yy, xx + 1]
-                half = LANES // 2
                 low = jnp.concatenate([even[:, :half], odd[:, :half]], axis=1)
                 high = jnp.concatenate([even[:, half:], odd[:, half:]], axis=1)
                 lines_of.append(jnp.concatenate([low, high], axis=0))
-        down = jnp.concatenate(lines_of, axis=1)
+        return jnp.concatenate(lines_of, axis=1)
+
+    def share(b, part, down):
+        taps = taps_all[b]
+        base = part * rows + HALO
+        conv = upped[pl.ds(base - 2, rows), :] * taps[0:1]
+        conv = conv + upped[pl.ds(base - 1, rows), :] * taps[1:2]
+        conv = conv + upped[pl.ds(base, rows), :] * taps[2:3]
+        end = conv[:, 2 * LANES :]
+        main = jax.nn.gelu(conv[:, LANES : 2 * LANES], approximate=True) * conv[:, :LANES]
+        rest = jax.nn.gelu(pltpu.roll(end, LANES // 2, 1), approximate=True) * end
+        hidden = jnp.concatenate([main, rest], axis=1).astype(jnp.bfloat16)
+        return jnp.dot(hidden[:, : down.shape[0]], down, preferred_element_type=jnp.float32)
+
+    def compute(i):
+        b = block(i)
+        project(b, 0, 2 * rows + HALO)
+        down = down_of(b)
         for part in (0, 1):
-            base = part * rows + HALO
-            conv = upped[pl.ds(base - 2, rows), :] * taps[0:1]
-            conv = conv + upped[pl.ds(base - 1, rows), :] * taps[1:2]
-            conv = conv + upped[pl.ds(base, rows), :] * taps[2:3]
-            end = conv[:, 2 * LANES :]
-            main = jax.nn.gelu(conv[:, LANES : 2 * LANES], approximate=True) * conv[:, :LANES]
-            rest = jax.nn.gelu(pltpu.roll(end, LANES // 2, 1), approximate=True) * end
-            hidden = jnp.concatenate([main, rest], axis=1).astype(jnp.bfloat16)
-            total[part] += jnp.dot(
-                hidden[:, : down.shape[0]], down, preferred_element_type=jnp.float32
-            )
-
+            total[part] += share(b, part, down)
+
+    down_x()
+    down_y(0)
+    first(jnp.int32(0), z)
     uz(1, z, to_zu)
     uz(2, z, to_zd)
-    dx_near, dx_far = dx_r.at[0], dx_r.at[1]
-    start(
-        moved(down_all.at[z, y, x], dxy_s, dx_near, to_xu),
-        moved(down_all.at[z, y, x], dxy_s, dx_near, to_xd),
-    )
-    first(jnp.int32(0), z)
+    down_z(0, 0)
+    last(jnp.int32(0), z, 0)
     own_rows = moved(rows_all.at[core], pair_s, pair_r, to_pair)
     own_rows.start()
     edge = pltpu.make_async_remote_copy(
         src_ref=rows_all.at[1, pl.ds(rows - HALO, HALO)], dst_ref=halo, send_sem=halo_s,
         recv_sem=halo_r, device_id=to_next, device_id_type=MESH,
     )
-    dy_near, dy_far = dy_r.at[0], dy_r.at[1]
 
     def normalize_rows():
         scale = norm_in_ref[...]
@@ -281,66 +317,131 @@
         before = normalized(halo[...].astype(jnp.float32), norm_in_ref[...])
         normed[0:HALO] = jnp.where(origin, 0.0, before).astype(jnp.bfloat16)
 
-    def turn(n, carry):
+    def turn(m, carry):
+        n = m - 4
+
         @pl.when(n == -4)
         def _():
-            landed(down_all.at[z, y, pl.ds(0, 2)], dx_near)
-            start(
-                moved(down_all.at[z, y, x_down, pl.ds(0, 48)], dxy_s, dx_far, to_xu),
-                moved(down_all.at[z, y, x_up, pl.ds(48, 48)], dxy_s, dx_far, to_xd),
-            )
-            pass_up(n + 5)
-            first(n + 5, block(n + 5))
+            down_landed(2, dx_r.at[0])
+            down_x_far()
+            down_y(1)
+            down_y(2)
 
         @pl.when(n == -3)
         def _():
-            landed(down_all.at[z, y, x], dx_far)
-            start(
-                moved(down_all.at[z, y], dxy_s, dy_near, to_yu),
-                moved(down_all.at[z, y], dxy_s, dy_near, to_yd),
-            )
-            send_down_line(0)
+            down_landed(1, dx_r.at[1])
+            down_y(3)
+            down_landed(4, dy_r.at[1])
+            down_y_far(1)
+            down_y_far(2)
+
+        @pl.when((n >= -3) & (n <= 0))
+        def _():
+            relay(2 * m - 1, block(2 * m - 1))
+
+        @pl.when(n <= -1)
+        def _():
+            relay(2 * m, block(2 * m))
+
+        @pl.when(n == -4)
+        def _():
+            down_landed(2, dy_r.at[0])
+            down_y_far(0)
+
+        @pl.when(n <= -1)
+        def _():
+            pass_up(2 * m + 1)
+            first(2 * m + 1, block(2 * m + 1))
+
+        @pl.when(n <= -2)
+        def _():
+            pass_up(2 * m + 2)
+            first(2 * m + 2, block(2 * m + 2))
+
+        @pl.when(n == -4)
+        def _():
+            down_z(0, 1, 2)
+            down_z(1, 0)
+            down_z(2, 0)
+
+        @pl.when(n == -3)
+        def _():
+            down_z(0, 3)
+            down_z(1, 1, 2)
+            down_z(2, 1, 2)
+            down_landed(1, dy_r.at[3])
+            down_z(3, 0)
 
         @pl.when(n == -2)
         def _():
-            landed(down_all.at[z, pl.ds(0, 2)], dy_near)
-            start(
-                moved(down_all.at[z, y_down, pl.ds(0, 2)], dxy_s, dy_far, to_yu),
-                moved(down_all.at[z, y_up, pl.ds(2, 2)], dxy_s, dy_far, to_yd),
-            )
-            send_down_line(1)
-            send_down_line(2)
+            down_landed(2, dy_r.at[2])
+            down_y_far(3)
+            down_z(1, 3)
+            down_z(2, 3)
+            down_landed(2, dy_r.at[4])
+            down_z(3, 1, 2)
 
         @pl.when(n == -1)
         def _():
-            landed(down_all.at[z, 0], dy_far)
-            send_down_line(3)
-
-        @pl.when(n + 6 < NZ)
-        def _():
-            pass_up(n + 6)
-            first(n + 6, block(n + 6))
-
-        @pl.when(n + 4 < NZ)
-        def _():
-            relay(n + 4, block(n + 4))
-
-        @pl.when((n >= -1) & (n + 1 < NZ))
-        def _():
-            hand_on(n + 1, block(n + 1), 1, 2)
-            hand_on(n + 1, block(n + 1), 3)
-
-        @pl.when((n >= -2) & (n + 2 < NZ))
-        def _():
-            hand_on(n + 2, block(n + 2), 0)
-
-        @pl.when((n >= -3) & (n + 3 < NZ))
+            down_landed(1, dy_r.at[5])
+            down_z(3, 3)
+
+        @pl.when((n >= -2) & (n < NZ - 3))
+        def _():
+            s = m // 2 - 1
+
+            @pl.when(lax.rem(m, 2) == 1)
+            def _():
+                pass_down(s + 1, 1)
+                pass_down(s + 1, 2)
+
+            @pl.when((lax.rem(m, 2) == 0) & (n > -2))
+            def _():
+                pass_down(s, 3)
+
+            @pl.when((lax.rem(m, 2) == 0) & (n < NZ - 4))
+            def _():
+                pass_down(s + 1, 0)
+
+        @pl.when(n == -3)
         def _():
             finish(n + 3, block(n + 3))
-
-        @pl.when(n + 4 < NZ)
+            hand_on(n + 3, block(n + 3), 0)
+            hand_on(n + 3, block(n + 3), 1, 2)
+
+        @pl.when((n == -2) | (n == -1))
+        def _():
+            finish(2 * m - 3, block(2 * m - 3))
+            finish(2 * m - 2, block(2 * m - 2))
+            hand_on(n + 2, block(n + 2), 3)
+
+        @pl.when((n >= 0) & (n + 5 < NZ))
+        def _():
+            finish(n + 5, block(n + 5))
+
+        @pl.when((n >= -2) & (n + 3 < NZ))
+        def _():
+            hand_on(n + 3, block(n + 3), 0)
+            hand_on(n + 3, block(n + 3), 1, 2)
+
+        @pl.when((n >= -1) & (n + 3 < NZ))
+        def _():
+            hand_on(n + 3, block(n + 3), 3)
+
+        @pl.when((n >= -3) & (n <= -1))
         def _():
             last(n + 4, block(n + 4), 0)
+
+        @pl.when(n <= -1)
+        def _():
+            last(n + 4, block(n + 4), 1)
+            last(n + 4, block(n + 4), 2)
+
+        @pl.when((n >= -1) & (n + 5 < NZ))
+        def _():
+            last(n + 5, block(n + 5), 0)
+            last(n + 5, block(n + 5), 1)
+            last(n + 5, block(n + 5), 2)
 
         @pl.when(n == -4)
         def _():
@@ -348,54 +449,50 @@
             edge.start()
             normalize_rows()
 
-        @pl.when(n == -1)
+        @pl.when(n == -2)
         def _():
             normalize_halo()
 
-        @pl.when((n >= 0) & (n < NZ - 2))
-        def _():
-            s = (n + 2) // 2
-
-            @pl.when(lax.rem(n, 2) == 0)
-            def _():
-                pass_down(s, 0)
-                pass_down(s, 1)
-
-            @pl.when(lax.rem(n, 2) == 1)
-            def _():
-                pass_down(s, 2)
-                pass_down(s, 3)
-
-        @pl.when(n == NZ - 1)
-        def _():
-            landed(down_all.at[0], dz_r.at[3, 0])
-
-        @pl.when(n >= 0)
-        def _():
-            complete(n, block(n))
-            compute(n)
+        @pl.when(n >= -1)
+        def _():
+            complete(n + 1, block(n + 1))
+            compute(n + 1)
 
         return carry
 
-    lax.fori_loop(-4, NZ, turn, jnp.int32(0))
+    lax.fori_loop(0, NZ + 2, turn, jnp.int32(0))
 
     pieces = 4
     size = rows // pieces
 
-    def piece(k, ref):
+    def piece(k):
         return pltpu.make_async_remote_copy(
-            src_ref=leaving.at[k], dst_ref=ref.at[k], send_sem=sum_s,
+            src_ref=leaving.at[k], dst_ref=arriving.at[k], send_sem=sum_s,
             recv_sem=sum_r.at[k], device_id=to_pair, device_id_type=MESH,
         )
 
-    for k in range(pieces):
-        leaving[k] = total[1 - core, pl.ds(k * size, size), :].astype(jnp.bfloat16)
-        if k:
-            piece(k - 1, arriving).start()
-    piece(pieces - 1, arriving).start()
+    i = jnp.int32(NZ - 1)
+    b = block(i)
+    landed(down_all.at[0], dz_r.at[3, 0])
+    complete(i, b)
+    for mine in (0, 1):
+        @pl.when(core == mine)
+        def _():
+            theirs = 1 - mine
+            project(b, theirs * rows, rows + HALO)
+            down = down_of(b)
+            ready = total[theirs] + share(b, theirs, down)
+            for k in range(pieces):
+                leaving[k] = ready[k * size : (k + 1) * size].astype(jnp.bfloat16)
+                if k:
+                    piece(k - 1).start()
+            project(b, mine * rows, rows + HALO)
+            piece(pieces - 1).start()
+            total[mine] += share(b, mine, down)
+
     out_scale = norm_out_ref[...]
     for k in range(pieces):
-        piece(k, arriving).wait_recv()
+        piece(k).wait_recv()
         whole = total[core, pl.ds(k * size, size), :] + arriving[k].astype(jnp.float32)
         out_ref[pl.ds(k * size, size), :] = normalized(whole, out_scale).astype(jnp.bfloat16)
 
@@ -440,7 +537,7 @@
         + [DMA((NZ - 1,))]
         + [DMA((NZ,))] * 2
         + [DMA((NZ, 3)), DMA((NZ,))]
-        + [DMA((2,))] * 2
+        + [DMA((2,)), DMA((6,))]
         + [DMA((4, 4)), DMA((4,))]
         + [DMA] * 5
         + [DMA((4,))],

time: 61.7 us -> 58.3 us (0.945)
  Pallas kernels: 59.7 us -> 56.2 us
    pallas_call x1, Pallas kernels: 59.7 us -> 56.2 us  [shards(): pl.pallas_call(kernel, in_specs=[hbm, vmem, hbm, hbm, vmem, vmem, hbm, vm...]
where the time goes in v5:
time: 58.3 us; the launch traced here: 58.1 us
  Pallas kernels  56.2 us (96%)
  local copies, waits for them, and re-layouts  1.87 us (3%)
    pallas_call x1, Pallas kernels, shards(): pl.pallas_call(kernel, in_specs=[hbm, vmem, hbm, hbm, vmem, vmem, hbm, vm...  56.2 us
    unnamed x1, local copies, waits for them, and re-layouts  1.87 us

profile of v5, /device:TPU:1, one launch (start us, length us, event | category | flops | bytes accessed | tf_op | source)
XLA Modules:
  0.0 58.1 jit_solution(3946972357570865922)
XLA Ops:
  0.0 56.2 %shard_map.82 = bf16[256,1024]{1,0:T(8,128)(2,1)} custom-call(bf16[256,1024]{1,0:T(8,128)(2,1)} %tokens_ref.1, f32[1,1024]{1,0:T(1,128)} %bitcast.4, bf16[64,176]{1,0:T(8,128)(2,1)} %value_ref.1, bf16[64,176]{1,0:T(8,128)(2,1)} %gate_ref.1, f32[3,176]{1,0:T(4,128)} %value_taps_ref.1, f32[3,176]{1,0:T(4,128)} %gate_taps_ref.1, bf16[64,176]{1,0:T(8,128)(2,1)} %bitcast.3, ...), custom_call_target="tpu_custom_call" | custom-call | tf_op jit(solution)/shard_map/pallas_call | solution.py:516
  56.2 1.9 %copy.10 = bf16[256,1024]{1,0:T(8,128)(2,1)} copy(bf16[256,1024]{1,0:T(8,128)(2,1)} %shard_map.82) | data formatting | bytes 1048576
